TPU v7x, 32 devices: a whole 2x2x4 slice. The times are simulated.
32 devices in a mesh: ep: 8 (over z, core), tp: 4 (over y, x).
Axes of the slice: x: 2, y: 2, z: 4, core: 2. Of those that a mesh axis runs over, the one named last changes fastest.
Arguments:
- residual: bfloat16 [512, 2048], P('ep', 'tp')
- state_re: float32 [512, 64, 64], P('ep', 'tp'), may hold values from -4 to 4
- state_im: float32 [512, 64, 64], P('ep', 'tp'), may hold values from -4 to 4
- mix_gain: float32 [2048], replicated, may hold values from 0.1 to 1.9
- proj_in: bfloat16 [2048, 1024], P(None, 'tp'), may hold values from -0.125 to 0.125
- decay_rate: float32 [64, 64], P('tp'), may hold values from 0.1 to 10
- frequency: float32 [64, 64], P('tp'), may hold values from 0 to 201.06177
- log_step: float32 [64], P('tp'), may hold values from -6.9078 to -2.3026
- input_re: float32 [64, 64, 16], P('tp'), may hold values from -1 to 1
- input_im: float32 [64, 64, 16], P('tp'), may hold values from -1 to 1
- read_re: float32 [64, 16, 64], P('tp'), may hold values from -0.5 to 0.5
- read_im: float32 [64, 16, 64], P('tp'), may hold values from -0.5 to 0.5
- skip_gain: float32 [1024], P('tp'), may hold values from -4 to 4
- glu_weight: bfloat16 [1024, 1024], P(None, 'tp'), may hold values from -0.1875 to 0.1875
- out_proj: bfloat16 [1024, 2048], P(None, 'tp'), may hold values from -0.1875 to 0.1875
- ffn_gain: float32 [2048], replicated, may hold values from 0.1 to 1.9
- router: float32 [2048, 8], replicated, may hold values from -0.125 to 0.125
- gate_weight: bfloat16 [8, 2048, 4096], P('ep', None, 'tp'), may hold values from -0.33007812 to 0.33007812
- up_weight: bfloat16 [8, 2048, 4096], P('ep', None, 'tp'), may hold values from -0.33007812 to 0.33007812
- down_weight: bfloat16 [8, 4096, 2048], P('ep', 'tp'), may hold values from -0.046875 to 0.046875
- route_ids: int32 [512, 4], P('ep'), may hold values from 0 to 7, all different within a row; in each aligned block of 64 rows (0 to 63, 64 to 127, ...) at most 33 rows name the same one
Outputs:
- layer_out: bfloat16 [512, 2048], P('ep', 'tp')
- state_re_new: float32 [512, 64, 64], P('ep', 'tp')
- state_im_new: float32 [512, 64, 64], P('ep', 'tp')
Inputs may be any that keep to these rules, and one draw needn't show every extreme that they name: `route_ids`: each row names 4 different experts. Within the rows of one ep index (aligned blocks of 64 rows) no expert is named more than 33 times, and in some block some expert is named exactly 33 times.
All inputs are finite; a program needn't handle non-finite values.
Results may differ from a plain program's by a relative error of at most 0.014.
Values may be sent and summed in bfloat16 or wider, within the bound.
A program may use at most 64 MiB of HBM per device.

v0:
```python
import functools

import jax
import jax.numpy as jnp
from jax import lax
from jax.experimental import pallas as pl
from jax.experimental.pallas import tpu as pltpu
from jax.sharding import PartitionSpec as P

EPSILON = 1e-05
LIMIT = 7.0
ALPHA = 1.702


def discretise(decay_rate, frequency, log_step, input_re, input_im):
    real_part = -decay_rate
    step_size = jnp.exp(log_step)[:, None]
    magnitude = jnp.exp(step_size * real_part)
    abar_re = magnitude * jnp.cos(step_size * frequency)
    abar_im = magnitude * jnp.sin(step_size * frequency)
    denom = real_part * real_part + frequency * frequency
    minus_one = abar_re - 1.0
    coef_re = (minus_one * real_part + abar_im * frequency) / denom
    coef_im = (abar_im * real_part - minus_one * frequency) / denom
    bbar_re = coef_re[..., None] * input_re - coef_im[..., None] * input_im
    bbar_im = coef_re[..., None] * input_im + coef_im[..., None] * input_re
    return (abar_re, abar_im, bbar_re, bbar_im)


def per_device(
    residual,
    state_re,
    state_im,
    mix_gain,
    proj_in,
    decay_rate,
    frequency,
    log_step,
    input_re,
    input_im,
    read_re,
    read_im,
    skip_gain,
    glu_weight,
    out_proj,
    ffn_gain,
    router,
    gate_weight,
    up_weight,
    down_weight,
    route_ids,
):
    high = lax.Precision.HIGHEST
    seq_rows = residual.shape[0]
    col_count = residual.shape[1]
    width = mix_gain.shape[0]
    ep_size = lax.axis_size("ep")
    own_resid = residual.astype(jnp.float32)
    full_resid = lax.all_gather(residual, "tp", axis=1, tiled=True).astype(jnp.float32)
    scale_one = lax.rsqrt(jnp.mean(full_resid * full_resid, axis=1, keepdims=True) + EPSILON)
    xnorm = (full_resid * scale_one * mix_gain).astype(jnp.bfloat16)
    mix_in = jnp.dot(xnorm, proj_in, preferred_element_type=jnp.float32).astype(jnp.bfloat16)
    mix_f = mix_in.astype(jnp.float32)
    group_count = decay_rate.shape[0]
    group_width = input_re.shape[2]
    grouped = mix_f.reshape(seq_rows, group_count, group_width)
    abar_re, abar_im, bbar_re, bbar_im = discretise(
        decay_rate, frequency, log_step, input_re, input_im
    )
    drive_re = jnp.einsum("sgc,gnc->sgn", grouped, bbar_re, precision=high)
    drive_im = jnp.einsum("sgc,gnc->sgn", grouped, bbar_im, precision=high)
    state_re_new = abar_re * state_re - abar_im * state_im + drive_re
    state_im_new = abar_re * state_im + abar_im * state_re + drive_im
    readout = jnp.einsum("sgn,gcn->sgc", state_re_new, read_re, precision=high) - jnp.einsum(
        "sgn,gcn->sgc", state_im_new, read_im, precision=high
    )
    mixer = jax.nn.gelu(
        readout.reshape(seq_rows, group_count * group_width) + skip_gain * mix_f, approximate=False
    )
    all_mixer = lax.all_gather(mixer.astype(jnp.bfloat16), "tp", axis=1, tiled=True)
    glu_gate = jnp.dot(all_mixer, glu_weight, preferred_element_type=jnp.float32)
    gated = (mixer * jax.nn.sigmoid(glu_gate)).astype(jnp.bfloat16)
    all_gated = lax.all_gather(gated, "tp", axis=1, tiled=True)
    mixed = jnp.dot(all_gated, out_proj, preferred_element_type=jnp.float32)
    stream = (own_resid + mixed).astype(jnp.bfloat16)
    stream_f = stream.astype(jnp.float32)
    all_stream = lax.all_gather(stream, "tp", axis=1, tiled=True).astype(jnp.float32)
    inverse = lax.rsqrt(jnp.mean(all_stream * all_stream, axis=1, keepdims=True) + EPSILON)
    logits = jnp.dot(all_stream * ffn_gain, router, precision=high) * inverse
    payload = (all_stream * inverse * ffn_gain).astype(jnp.bfloat16)
    expert_count = router.shape[1]
    top_count = route_ids.shape[1]
    capacity = seq_rows * top_count // expert_count + 1
    expert_iota = jnp.arange(expert_count, dtype=jnp.int32)
    choose = (route_ids[:, :, None] == expert_iota).astype(jnp.float32)
    picked = jnp.sum(choose * logits[:, None, :], axis=2)
    expon = jnp.exp(picked)
    weights = expon / jnp.sum(expon, axis=1, keepdims=True)
    flat_route = route_ids.reshape(seq_rows * top_count)
    one_hot = (flat_route[:, None] == expert_iota).astype(jnp.int32)
    before = jnp.cumsum(one_hot, axis=0) - one_hot
    slot_ids = jnp.sum(before * one_hot, axis=1)
    target = flat_route * capacity + slot_ids
    slot_iota = jnp.arange(expert_count * capacity, dtype=jnp.int32)
    placing = jnp.any(slot_iota[:, None, None] == target.reshape(seq_rows, top_count)[None], axis=2)
    buffer = jnp.dot(placing.astype(jnp.bfloat16), payload, preferred_element_type=jnp.float32)
    buffer = buffer.astype(jnp.bfloat16).reshape(expert_count, capacity, payload.shape[1])
    local_experts = gate_weight.shape[0]
    received = lax.all_to_all(buffer, "ep", split_axis=0, concat_axis=0, tiled=True)
    items = received.shape[1]
    tokens = received.reshape(ep_size, local_experts, items, width)
    tokens = tokens.transpose(1, 0, 2, 3).reshape(local_experts, ep_size * items, width)
    gate_pre = jnp.einsum("esd,edf->esf", tokens, gate_weight, preferred_element_type=jnp.float32)
    up_pre = jnp.einsum("esd,edf->esf", tokens, up_weight, preferred_element_type=jnp.float32)
    gate_cl = jnp.minimum(gate_pre, LIMIT)
    up_cl = jnp.clip(up_pre, -LIMIT, LIMIT)
    active = ((up_cl + 1.0) * (gate_cl * jax.nn.sigmoid(ALPHA * gate_cl))).astype(jnp.bfloat16)
    partial_value = jnp.einsum(
        "esf,efd->esd", active, down_weight, preferred_element_type=jnp.float32
    ).astype(jnp.bfloat16)
    summed = lax.psum_scatter(
        partial_value.astype(jnp.float32).astype(jnp.bfloat16),
        "tp",
        scatter_dimension=2,
        tiled=True,
    )
    outgoing = summed.reshape(local_experts, ep_size, items, col_count)
    outgoing = outgoing.transpose(1, 0, 2, 3).reshape(ep_size * local_experts, items, col_count)
    returned = lax.all_to_all(outgoing, "ep", split_axis=0, concat_axis=0, tiled=True)
    flat_back = returned.reshape(expert_count * capacity, col_count)
    fetched = (
        jnp.take(flat_back, target, axis=0)
        .astype(jnp.float32)
        .reshape(seq_rows, top_count, col_count)
    )
    experts_sum = jnp.sum(weights[..., None] * fetched, axis=1)
    layer_out = (stream_f + experts_sum).astype(jnp.bfloat16)
    return (layer_out, state_re_new, state_im_new)


def erf(x):
    x = jnp.clip(x, -3.832506856900711, 3.832506856900711)
    y = x * x
    top = 0.00022905065861350646
    for coefficient in (
        0.0034082910107109506,
        0.050955695062380861,
        0.18520832239976145,
        1.128379143519084,
    ):
        top = top * y + coefficient
    bottom = -1.1791602954361697e-7
    for coefficient in (
        0.000023547966471313185,
        0.0010179625278914885,
        0.014070470171167667,
        0.11098505178285362,
        0.49746925110067538,
        1.0,
    ):
        bottom = bottom * y + coefficient
    return x * top / bottom


def layer_kernel(
    sizes,
    resid_ref,
    gain1_ref,
    decay_ref,
    freq_ref,
    step_ref,
    in_re_ref,
    in_im_ref,
    read_re_ref,
    read_im_ref,
    skip_ref,
    gain2_ref,
    router_ref,
    route_ref,
    sre_hbm,
    sim_hbm,
    proj_hbm,
    glu_hbm,
    outp_hbm,
    gate_hbm,
    up_hbm,
    down_hbm,
    out_ref,
    sre_out,
    sim_out,
    sre,
    sim,
    proj,
    glu,
    outp,
    wg,
    wu,
    wd,
    res_all,
    mix_all,
    gated_all,
    logit_all,
    buf,
    recv,
    tok_all,
    acc_g,
    acc_u,
    part_out,
    part_in,
    unpack,
    repack,
    back,
    fin,
    load_sem,
    store_sem,
    tp_send,
    tp_recv,
    ep_send,
    ep_recv,
):
    ep, tp, cap, packed, rows = sizes
    f32, bf16 = jnp.float32, jnp.bfloat16
    me, t = lax.axis_index("ep"), lax.axis_index("tp")
    seqs, cols = resid_ref.shape
    width = cols * tp
    groups, states = decay_ref.shape
    chans = skip_ref.shape[1]
    group_width = chans // groups
    chunks = cols // 128
    items = ep * packed

    def dot(a, b):
        return jnp.dot(a, b, preferred_element_type=f32)

    loads = [
        pltpu.make_async_copy(a, b, load_sem.at[n])
        for n, (a, b) in enumerate(
            [
                (proj_hbm, proj),
                (sre_hbm, sre),
                (sim_hbm, sim),
                (glu_hbm, glu),
                (outp_hbm, outp),
                (gate_hbm, wg),
                (up_hbm, wu),
            ]
            + [(down_hbm.at[:, j * cols : (j + 1) * cols], wd.at[j]) for j in range(tp)]
        )
    ]
    for load in loads:
        load.start()

    barrier = pltpu.get_barrier_semaphore()
    for k in range(1, tp):
        pl.semaphore_signal(barrier, inc=1, device_id=(me, (t + k) % tp), device_id_type=pl.DeviceIdType.MESH)
    for k in range(1, ep):
        pl.semaphore_signal(barrier, inc=1, device_id=((me + k) % ep, t), device_id_type=pl.DeviceIdType.MESH)
    pl.semaphore_wait(barrier, tp + ep - 2)

    def tp_copy(phase, k, source, target):
        return pltpu.make_async_remote_copy(
            src_ref=source,
            dst_ref=target,
            send_sem=tp_send.at[phase, k],
            recv_sem=tp_recv.at[phase, k],
            device_id=(me, (t + k) % tp),
            device_id_type=pl.DeviceIdType.MESH,
        )

    def ep_copy(phase, k, source, target):
        return pltpu.make_async_remote_copy(
            src_ref=source,
            dst_ref=target,
            send_sem=ep_send.at[phase, k],
            recv_sem=ep_recv.at[phase, k],
            device_id=((me + k) % ep, t),
            device_id_type=pl.DeviceIdType.MESH,
        )

    order = [2, 1, 3] if tp == 4 else list(range(1, tp))
    gather0 = [tp_copy(0, k, resid_ref, res_all.at[t]) for k in range(1, tp)]
    for copy in gather0:
        copy.start()
    res_all[t] = resid_ref[...]

    square = (groups, groups)
    diagonal = lax.broadcasted_iota(jnp.int32, square, 0) == lax.broadcasted_iota(jnp.int32, square, 1)
    log_step = jnp.sum(
        jnp.where(diagonal, jnp.broadcast_to(step_ref[...], square), 0.0), axis=1, keepdims=True
    )
    step_size = jnp.exp(log_step)
    real_part, imag_part = -decay_ref[...], freq_ref[...]
    magnitude = jnp.exp(step_size * real_part)
    abar_re = magnitude * jnp.cos(step_size * imag_part)
    abar_im = magnitude * jnp.sin(step_size * imag_part)
    denom = real_part * real_part + imag_part * imag_part
    minus_one = abar_re - 1.0
    coef_re = ((minus_one * real_part + abar_im * imag_part) / denom)[:, None, :]
    coef_im = ((abar_im * real_part - minus_one * imag_part) / denom)[:, None, :]
    in_re, in_im = in_re_ref[...], in_im_ref[...]
    bb_re = (coef_re * in_re - coef_im * in_im).astype(bf16).reshape(chans, states)
    bb_im = (coef_re * in_im + coef_im * in_re).astype(bf16).reshape(chans, states)
    abar_re, abar_im = abar_re[None], abar_im[None]

    route = route_ref[...]
    iota_e = lax.broadcasted_iota(jnp.int32, (ep, seqs), 0)
    routed_t = jnp.zeros((ep, seqs), f32)
    for j in range(route.shape[0]):
        routed_t = routed_t + jnp.where(route[j : j + 1, :] == iota_e, 1.0, 0.0)
    row_i = lax.broadcasted_iota(jnp.int32, (seqs, seqs), 0)
    col_i = lax.broadcasted_iota(jnp.int32, (seqs, seqs), 1)
    routed_h = routed_t.astype(bf16)
    earlier_t = dot(routed_h, jnp.where(row_i < col_i, 1.0, 0.0).astype(bf16))
    place_t = jnp.where(routed_t > 0.5, earlier_t, -1000.0)
    last = (((1,), (1,)), ((), ()))
    earlier = lax.dot_general(
        jnp.where(col_i < row_i, 1.0, 0.0).astype(bf16), routed_h, last, preferred_element_type=f32
    )
    routed = lax.dot_general(
        jnp.where(row_i == col_i, 1.0, 0.0).astype(bf16), routed_h, last, preferred_element_type=f32
    )
    place = jnp.where(routed > 0.5, earlier, -1000.0)
    lane = lax.broadcasted_iota(jnp.int32, (1, items), 1)
    owner = jnp.zeros((1, items), jnp.int32)
    for p in range(1, ep):
        owner = owner + jnp.where(lane >= p * packed, 1, 0)
    within = lane - owner * packed
    iota_q = lax.broadcasted_iota(jnp.int32, (rows, items), 0)
    for c in range(chunks):
        d = within - c * cap
        value = jnp.where((d >= 0) & (d < cap), owner * cap + d, -1)
        unpack[c] = jnp.where(iota_q == value, 1.0, 0.0).astype(bf16)
    iota_r = lax.broadcasted_iota(jnp.int32, (packed, rows), 0)
    iota_l = lax.broadcasted_iota(jnp.int32, (packed, rows), 1)
    for c in range(chunks):
        d = iota_r - c * cap
        value = jnp.where((d >= 0) & (d < cap), d, -5000)
        for p in range(ep):
            repack[c, p * packed : (p + 1) * packed, :] = jnp.where(
                iota_l - p * cap == value, 1.0, 0.0
            ).astype(bf16)

    loads[0].wait()
    for copy in gather0:
        copy.wait_recv()
    total = jnp.zeros((seqs, 1), f32)
    for j in range(tp):
        part = res_all[j].astype(f32)
        total = total + jnp.sum(part * part, axis=1, keepdims=True)
    scale = lax.rsqrt(total / width + EPSILON)
    mix = jnp.zeros((seqs, chans), f32)
    for j in range(tp):
        xnorm = (res_all[j].astype(f32) * scale * gain1_ref[j]).astype(bf16)
        mix = mix + dot(xnorm, proj[j * cols : (j + 1) * cols, :])
    mix_f = mix.astype(bf16).astype(f32)
    lane_c = lax.broadcasted_iota(jnp.int32, (seqs, groups, chans), 2)
    group_c = lax.broadcasted_iota(jnp.int32, (seqs, groups, chans), 1)
    first = group_c * group_width
    own = (lane_c >= first) & (lane_c < first + group_width)
    spread = jnp.where(own, jnp.broadcast_to(mix_f[:, None, :], own.shape), 0.0)
    spread = spread.astype(bf16).reshape(seqs * groups, chans)
    drive_re = dot(spread, bb_re).reshape(seqs, groups, states)
    drive_im = dot(spread, bb_im).reshape(seqs, groups, states)
    loads[1].wait()
    loads[2].wait()
    old_re, old_im = sre[...], sim[...]
    new_re = abar_re * old_re - abar_im * old_im + drive_re
    new_im = abar_re * old_im + abar_im * old_re + drive_im
    sre[...] = new_re
    sim[...] = new_im
    stores = [
        pltpu.make_async_copy(sre, sre_out, store_sem.at[0]),
        pltpu.make_async_copy(sim, sim_out, store_sem.at[1]),
    ]
    for store in stores:
        store.start()
    flat = (seqs * groups, states)
    readout = lax.dot_general(
        new_re.reshape(flat).astype(bf16), read_re_ref[...].astype(bf16), last, preferred_element_type=f32
    ) - lax.dot_general(
        new_im.reshape(flat).astype(bf16), read_im_ref[...].astype(bf16), last, preferred_element_type=f32
    )
    readout = jnp.sum(jnp.where(own, readout.reshape(seqs, groups, chans), 0.0), axis=1)
    pre = readout + skip_ref[...] * mix_f
    mixer = 0.5 * pre * (1.0 + erf(pre * 0.7071067811865476))
    mix_all[t] = mixer.astype(bf16)
    gather1 = [tp_copy(1, k, mix_all.at[t], mix_all.at[t]) for k in range(1, tp)]
    for copy in gather1:
        copy.start()
    loads[3].wait()
    for copy in gather1:
        copy.wait_recv()
    glu_gate = jnp.zeros((seqs, chans), f32)
    for j in range(tp):
        glu_gate = glu_gate + dot(mix_all[j], glu[j * chans : (j + 1) * chans, :])
    gated_all[t] = (mixer * jax.nn.sigmoid(glu_gate)).astype(bf16)
    gather2 = [tp_copy(2, k, gated_all.at[t], gated_all.at[t]) for k in range(1, tp)]
    for copy in gather2:
        copy.start()
    loads[4].wait()
    for copy in gather2:
        copy.wait_recv()
    mixed = resid_ref[...].astype(f32)
    for j in range(tp):
        mixed = mixed + dot(gated_all[j], outp[j * chans : (j + 1) * chans, :])
    stream = mixed.astype(bf16)
    stream_f = stream.astype(f32)

    iota_p = lax.broadcasted_iota(jnp.int32, (ep, packed, seqs), 1).astype(f32)
    place_b = jnp.broadcast_to(place_t[:, None, :], (ep, packed, seqs))
    tokens = jnp.zeros((items, 128), f32)
    for c in range(chunks):
        choose = jnp.where(iota_p - c * cap == place_b, 1.0, 0.0)
        tokens = tokens + dot(
            choose.astype(bf16).reshape(items, seqs), stream[:, c * 128 : (c + 1) * 128]
        )
    buf[...] = tokens.astype(bf16).reshape(ep, packed, 128)
    sends = [ep_copy(0, k, buf.at[(me + k) % ep], recv.at[me]) for k in range(1, ep)]
    for copy in sends:
        copy.start()
    recv[me] = buf[me]

    logit_all[t] = jnp.zeros(logit_all.shape[1:], f32)
    logit_all[t, :, 0:ep] = lax.dot_general(
        stream_f * gain2_ref[t],
        router_ref[:, pl.ds(pl.multiple_of(t * cols, cols), cols)],
        last,
        precision=lax.Precision.HIGHEST,
        preferred_element_type=f32,
    )
    logit_all[t, :, ep : ep + 1] = jnp.sum(stream_f * stream_f, axis=1, keepdims=True)
    gather3 = [tp_copy(3, k, logit_all.at[t], logit_all.at[t]) for k in range(1, tp)]
    for copy in gather3:
        copy.start()

    for copy in sends:
        copy.wait_recv()
    received = recv[...].reshape(items, 128)
    for c in range(chunks):
        tok_all[t, :, c * 128 : (c + 1) * 128] = dot(unpack[c], received).astype(bf16)
    beside, across = t + 1 - 2 * (t % 2), (t + 2) % tp
    opposite = (beside + 2) % tp
    half = rows // 32 * 16

    def side_copy(phase, n, block, peer):
        return pltpu.make_async_remote_copy(
            src_ref=block,
            dst_ref=block,
            send_sem=tp_send.at[phase, n],
            recv_sem=tp_recv.at[phase, n],
            device_id=(me, peer),
            device_id_type=pl.DeviceIdType.MESH,
        )

    gather4 = [
        side_copy(4, 0, tok_all.at[t], beside),
        side_copy(4, 1, tok_all.at[t], across),
        side_copy(4, 2, tok_all.at[beside, pl.ds(0, half)], across),
        side_copy(4, 3, tok_all.at[across, pl.ds(half, rows - half)], beside),
    ]
    gather4[0].start()
    gather4[1].start()

    for copy in gather3:
        copy.wait_recv()
    summed = logit_all[0]
    for j in range(1, tp):
        summed = summed + logit_all[j]
    inverse = lax.rsqrt(summed[:, ep : ep + 1] / width + EPSILON)
    logits = summed[:, 0:ep] * inverse
    chosen = routed > 0.5
    expon = jnp.where(chosen, jnp.exp(jnp.where(chosen, logits, 0.0)), 0.0)
    weights = expon / jnp.sum(expon, axis=1, keepdims=True)

    loads[5].wait()
    loads[6].wait()
    squares = jnp.zeros((rows, 1), f32)
    for n, j in enumerate([t, beside, across, opposite]):
        if n == 1:
            gather4[0].wait_recv()
            gather4[2].start()
            gather4[1].wait_recv()
            gather4[3].start()
        if n == 3:
            gather4[2].wait_recv()
            gather4[3].wait_recv()
        part = tok_all[j].astype(f32)
        squares = squares + jnp.sum(part * part, axis=1, keepdims=True)
        scaled = (part * gain2_ref[j]).astype(bf16)
        span = pl.ds(pl.multiple_of(j * cols, cols), cols)
        if n == 0:
            acc_g[...] = dot(scaled, wg[span, :])
            acc_u[...] = dot(scaled, wu[span, :])
        else:
            acc_g[...] += dot(scaled, wg[span, :])
            acc_u[...] += dot(scaled, wu[span, :])
    norm = lax.rsqrt(squares / width + EPSILON)
    gate_cl = jnp.minimum(acc_g[...] * norm, LIMIT)
    up_cl = jnp.clip(acc_u[...] * norm, -LIMIT, LIMIT)
    active = ((up_cl + 1.0) * (gate_cl * jax.nn.sigmoid(ALPHA * gate_cl))).astype(bf16)
    for load in loads[7:]:
        load.wait()
    scatter = {k: tp_copy(5, k, part_out.at[k], part_in.at[k]) for k in range(1, tp)}
    for k in order:
        part_out[k] = dot(active, wd[(t + k) % tp]).astype(bf16)
        scatter[k].start()
    result = dot(active, wd[t]).astype(bf16).astype(f32)

    expand = jnp.where(lax.broadcasted_iota(jnp.int32, (ep, items), 0) == owner, 1.0, 0.0).astype(bf16)
    place_x = dot(place.astype(bf16), expand)
    weight_x = dot(weights.astype(bf16), expand)
    within_f = within.astype(f32)
    combine = [
        jnp.where(within_f - c * cap == place_x, weight_x, 0.0).astype(bf16) for c in range(chunks)
    ]
    for k in order:
        scatter[k].wait_recv()
        result = result + part_in[k].astype(f32)
    result = result.astype(bf16)
    outgoing = jnp.zeros((items, 128), f32)
    for c in range(chunks):
        outgoing = outgoing + dot(repack[c], result[:, c * 128 : (c + 1) * 128])
    back[...] = outgoing.astype(bf16).reshape(ep, packed, 128)
    returns = [ep_copy(1, k, back.at[(me + k) % ep], fin.at[me]) for k in range(1, ep)]
    for copy in returns:
        copy.start()
    fin[me] = back[me]
    for copy in returns:
        copy.wait_recv()
    final = fin[...].reshape(items, 128)
    for c in range(chunks):
        span = slice(c * 128, (c + 1) * 128)
        out_ref[:, span] = (stream_f[:, span] + dot(combine[c], final)).astype(bf16)
    for copy in gather0 + gather1 + gather2 + gather3 + sends + returns:
        copy.wait_send()
    for k in order:
        scatter[k].wait_send()
    for copy in gather4:
        copy.wait_send()
    for store in stores:
        store.wait()


def finish_kernel(a_in, b_in, c_in, a_out, b_out, c_out, a, b, c, sems):
    reads = [
        pltpu.make_async_copy(source, held, sems.at[n])
        for n, (source, held) in enumerate(((a_in, a), (b_in, b), (c_in, c)))
    ]
    writes = [
        pltpu.make_async_copy(held, target, sems.at[3 + n])
        for n, (held, target) in enumerate(((a, a_out), (b, b_out), (c, c_out)))
    ]
    for read in reads:
        read.start()
    for read, write in zip(reads, writes):
        read.wait()
        write.start()
    for write in writes:
        write.wait()


def dispatch(*args):
    (
        residual, state_re, state_im, mix_gain, proj_in, decay_rate, frequency, log_step,
        input_re, input_im, read_re, read_im, skip_gain, glu_weight, out_proj, ffn_gain,
        router, gate_weight, up_weight, down_weight, route_ids,
    ) = args
    ep, tp = lax.axis_size("ep"), lax.axis_size("tp")
    seqs, cols = residual.shape
    groups, states = decay_rate.shape
    chans = skip_gain.shape[0]
    if gate_weight.shape[0] != 1 or groups % 16 or chans % 128 or cols % 128 or tp != 4 or seqs % 16:
        return per_device(*args)
    top = route_ids.shape[1]
    cap = seqs * top // router.shape[1] + 1
    packed = -(-cap * (cols // 128) // 16) * 16
    rows = -(-ep * cap // 16) * 16
    hidden = gate_weight.shape[2]
    items = ep * packed
    bf16, f32 = jnp.bfloat16, jnp.float32
    vmem, anywhere = pl.BlockSpec(memory_space=pltpu.VMEM), pl.BlockSpec(memory_space=pl.ANY)
    state_shape = (seqs, groups, states)
    out = pl.pallas_call(
        functools.partial(layer_kernel, (ep, tp, cap, packed, rows)),
        out_shape=(
            jax.ShapeDtypeStruct((seqs, cols), bf16),
            jax.ShapeDtypeStruct(state_shape, f32),
            jax.ShapeDtypeStruct(state_shape, f32),
        ),
        in_specs=[vmem] * 13 + [anywhere] * 8,
        out_specs=(vmem, anywhere, anywhere),
        scratch_shapes=[
            pltpu.VMEM(state_shape, f32),
            pltpu.VMEM(state_shape, f32),
            pltpu.VMEM(proj_in.shape, bf16),
            pltpu.VMEM(glu_weight.shape, bf16),
            pltpu.VMEM(out_proj.shape, bf16),
            pltpu.VMEM(gate_weight.shape[1:], bf16),
            pltpu.VMEM(up_weight.shape[1:], bf16),
            pltpu.VMEM((tp, hidden, cols), bf16),
            pltpu.VMEM((tp, seqs, cols), bf16),
            pltpu.VMEM((tp, seqs, chans), bf16),
            pltpu.VMEM((tp, seqs, chans), bf16),
            pltpu.VMEM((tp, seqs, 128), f32),
            pltpu.VMEM((ep, packed, 128), bf16),
            pltpu.VMEM((ep, packed, 128), bf16),
            pltpu.VMEM((tp, rows, cols), bf16),
            pltpu.VMEM((rows, hidden), f32),
            pltpu.VMEM((rows, hidden), f32),
            pltpu.VMEM((tp, rows, cols), bf16),
            pltpu.VMEM((tp, rows, cols), bf16),
            pltpu.VMEM((cols // 128, rows, items), bf16),
            pltpu.VMEM((cols // 128, items, rows), bf16),
            pltpu.VMEM((ep, packed, 128), bf16),
            pltpu.VMEM((ep, packed, 128), bf16),
            pltpu.SemaphoreType.DMA((7 + tp,)),
            pltpu.SemaphoreType.DMA((2,)),
            pltpu.SemaphoreType.DMA((6, tp)),
            pltpu.SemaphoreType.DMA((6, tp)),
            pltpu.SemaphoreType.DMA((2, ep)),
            pltpu.SemaphoreType.DMA((2, ep)),
        ],
        compiler_params=pltpu.CompilerParams(
            collective_id=0, has_side_effects=True, vmem_limit_bytes=60 * 1024 * 1024
        ),
        name="layer",
    )(
        residual,
        mix_gain.reshape(tp, 1, cols),
        decay_rate,
        frequency,
        log_step.reshape(1, groups),
        input_re.transpose(0, 2, 1),
        input_im.transpose(0, 2, 1),
        read_re.reshape(chans, states),
        read_im.reshape(chans, states),
        skip_gain.reshape(1, chans),
        ffn_gain.reshape(tp, 1, cols),
        router.T,
        route_ids.T,
        state_re,
        state_im,
        proj_in,
        glu_weight,
        out_proj,
        gate_weight.reshape(gate_weight.shape[1:]),
        up_weight.reshape(up_weight.shape[1:]),
        down_weight.reshape(down_weight.shape[1:]),
    )
    return pl.pallas_call(
        finish_kernel,
        out_shape=tuple(jax.ShapeDtypeStruct(part.shape, part.dtype) for part in out),
        in_specs=[anywhere] * 3,
        out_specs=(anywhere,) * 3,
        scratch_shapes=[pltpu.VMEM(part.shape, part.dtype) for part in out]
        + [pltpu.SemaphoreType.DMA((6,))],
        name="finish",
    )(*out)


def solution(mesh):
    in_specs = (
        P("ep", "tp"),
        P("ep", "tp", None),
        P("ep", "tp", None),
        P(),
        P(None, "tp"),
        P("tp", None),
        P("tp", None),
        P("tp"),
        P("tp", None, None),
        P("tp", None, None),
        P("tp", None, None),
        P("tp", None, None),
        P("tp"),
        P(None, "tp"),
        P(None, "tp"),
        P(),
        P(),
        P("ep", None, "tp"),
        P("ep", None, "tp"),
        P("ep", "tp", None),
        P("ep", None),
    )
    out_specs = (P("ep", "tp"), P("ep", "tp", None), P("ep", "tp", None))
    return jax.shard_map(
        dispatch, mesh=mesh, in_specs=in_specs, out_specs=out_specs, check_vma=False
    )
```

profile of v0, /device:TPU:0, one launch (start us, length us, event | category | flops | bytes accessed | tf_op | source)
XLA Modules:
  0.0 67.3 jit_solution(16579977541001862932)
XLA Ops:
  0.6 64.5 %layer.1 = (bf16[64,512]{1,0:T(8,128)(2,1)}, f32[64,16,64]{2,1,0:T(8,128)}, f32[64,16,64]{2,1,0:T(8,128)}) custom-call(bf16[64,512]{1,0:T(8,128)(2,1)} %resid_ref.1, f32[4,1,512]{2,1,0:T(1,128)} %bitcast.21, f32[16,64]{1,0:T(8,128)} %decay_ref.1, f32[16,64]{1,0:T(8,128)} %freq_ref.1, f32[1,16]{1,0:T(1,128)} %bitcast.25, f32[16,16,64]{2,1,0:T(8,128)} %bitcast.16, ...), custom_call_target="tpu_custom_call" | custom-call | tf_op jit(solution)/shard_map/layer/pallas_call | solution.py:583
  65.2 2.1 %finish.1 = (bf16[64,512]{1,0:T(8,128)(2,1)}, f32[64,16,64]{2,1,0:T(8,128)}, f32[64,16,64]{2,1,0:T(8,128)}) custom-call(bf16[64,512]{1,0:T(8,128)(2,1)} %get-tuple-element.6.a_in, f32[64,16,64]{2,1,0:T(8,128)} %get-tuple-element.7.b_in, f32[64,16,64]{2,1,0:T(8,128)} %get-tuple-element.8.c_in), custom_call_target="tpu_custom_call" | custom-call | tf_op jit(solution)/shard_map/finish/pallas_call | solution.py:650
where the time goes:
time: 67.4 us; the launch traced here: 67.3 us
  Pallas kernels  66.6 us (99%)
    pallas_call x1, Pallas kernels, dispatch(): pl.pallas_call(functools.partial(layer_kernel, (ep, tp, cap, packed, rows...  64.5 us
    pallas_call x1, Pallas kernels, dispatch(): pl.pallas_call(finish_kernel, out_shape=tuple((jax.ShapeDtypeStruct(part....  2.1 us

commit v1 on v0

--- a/solution.py
+++ b/solution.py
@@ -200,25 +200,29 @@
     mix_all,
     gated_all,
     logit_all,
-    buf,
-    recv,
-    tok_all,
+    place_all,
+    weight_all,
+    pick,
+    spill,
+    tok,
     acc_g,
     acc_u,
-    part_out,
-    part_in,
-    unpack,
-    repack,
-    back,
-    fin,
+    act,
+    mine,
+    sib_out,
+    sib_in,
+    summed,
+    from_side,
+    fwd_in,
+    fwd_out,
+    home_out,
+    home_in,
     load_sem,
     store_sem,
-    tp_send,
-    tp_recv,
-    ep_send,
-    ep_recv,
+    send_sem,
+    recv_sem,
 ):
-    ep, tp, cap, packed, rows = sizes
+    ep, tp, cap, rows = sizes
     f32, bf16 = jnp.float32, jnp.bfloat16
     me, t = lax.axis_index("ep"), lax.axis_index("tp")
     seqs, cols = resid_ref.shape
@@ -226,8 +230,10 @@
     groups, states = decay_ref.shape
     chans = skip_ref.shape[1]
     group_width = chans // groups
-    chunks = cols // 128
-    items = ep * packed
+    chips = ep // 2
+    pair = 2 * seqs
+    half = seqs // 2
+    last = (((1,), (1,)), ((), ()))
 
     def dot(a, b):
         return jnp.dot(a, b, preferred_element_type=f32)
@@ -257,30 +263,37 @@
         pl.semaphore_signal(barrier, inc=1, device_id=((me + k) % ep, t), device_id_type=pl.DeviceIdType.MESH)
     pl.semaphore_wait(barrier, tp + ep - 2)
 
-    def tp_copy(phase, k, source, target):
-        return pltpu.make_async_remote_copy(
+    copies = []
+
+    def remote(source, target, peer):
+        n = len(copies)
+        copy = pltpu.make_async_remote_copy(
             src_ref=source,
             dst_ref=target,
-            send_sem=tp_send.at[phase, k],
-            recv_sem=tp_recv.at[phase, k],
-            device_id=(me, (t + k) % tp),
+            send_sem=send_sem.at[n],
+            recv_sem=recv_sem.at[n],
+            device_id=peer,
             device_id_type=pl.DeviceIdType.MESH,
         )
-
-    def ep_copy(phase, k, source, target):
-        return pltpu.make_async_remote_copy(
-            src_ref=source,
-            dst_ref=target,
-            send_sem=ep_send.at[phase, k],
-            recv_sem=ep_recv.at[phase, k],
-            device_id=((me + k) % ep, t),
-            device_id_type=pl.DeviceIdType.MESH,
-        )
-
-    order = [2, 1, 3] if tp == 4 else list(range(1, tp))
-    gather0 = [tp_copy(0, k, resid_ref, res_all.at[t]) for k in range(1, tp)]
-    for copy in gather0:
         copy.start()
+        copies.append(copy)
+        return copy
+
+    def flip(value, k):
+        for bit in (1, 2, 4, 8, 16):
+            if k & bit:
+                value = value + bit - 2 * bit * ((value // bit) % 2)
+        return value
+
+    beside, across = flip(t, 1), flip(t, 2)
+    opposite = flip(beside, 2)
+    sibling = flip(me, 1)
+    side_b, side_a, twin = (me, beside), (me, across), (sibling, t)
+
+    def gather(source, target):
+        return [remote(source, target, (me, flip(t, k))) for k in (3, 1, 2)]
+
+    gather0 = gather(resid_ref, res_all.at[t])
     res_all[t] = resid_ref[...]
 
     square = (groups, groups)
@@ -309,36 +322,13 @@
         routed_t = routed_t + jnp.where(route[j : j + 1, :] == iota_e, 1.0, 0.0)
     row_i = lax.broadcasted_iota(jnp.int32, (seqs, seqs), 0)
     col_i = lax.broadcasted_iota(jnp.int32, (seqs, seqs), 1)
-    routed_h = routed_t.astype(bf16)
-    earlier_t = dot(routed_h, jnp.where(row_i < col_i, 1.0, 0.0).astype(bf16))
-    place_t = jnp.where(routed_t > 0.5, earlier_t, -1000.0)
-    last = (((1,), (1,)), ((), ()))
-    earlier = lax.dot_general(
-        jnp.where(col_i < row_i, 1.0, 0.0).astype(bf16), routed_h, last, preferred_element_type=f32
-    )
-    routed = lax.dot_general(
-        jnp.where(row_i == col_i, 1.0, 0.0).astype(bf16), routed_h, last, preferred_element_type=f32
-    )
-    place = jnp.where(routed > 0.5, earlier, -1000.0)
-    lane = lax.broadcasted_iota(jnp.int32, (1, items), 1)
-    owner = jnp.zeros((1, items), jnp.int32)
-    for p in range(1, ep):
-        owner = owner + jnp.where(lane >= p * packed, 1, 0)
-    within = lane - owner * packed
-    iota_q = lax.broadcasted_iota(jnp.int32, (rows, items), 0)
-    for c in range(chunks):
-        d = within - c * cap
-        value = jnp.where((d >= 0) & (d < cap), owner * cap + d, -1)
-        unpack[c] = jnp.where(iota_q == value, 1.0, 0.0).astype(bf16)
-    iota_r = lax.broadcasted_iota(jnp.int32, (packed, rows), 0)
-    iota_l = lax.broadcasted_iota(jnp.int32, (packed, rows), 1)
-    for c in range(chunks):
-        d = iota_r - c * cap
-        value = jnp.where((d >= 0) & (d < cap), d, -5000)
-        for p in range(ep):
-            repack[c, p * packed : (p + 1) * packed, :] = jnp.where(
-                iota_l - p * cap == value, 1.0, 0.0
-            ).astype(bf16)
+    earlier_t = dot(routed_t.astype(bf16), jnp.where(row_i < col_i, 1.0, 0.0).astype(bf16))
+    place_all[0, 0] = jnp.zeros(place_all.shape[2:], f32)
+    place_all[0, 0, :, 0:seqs] = jnp.where(routed_t > 0.5, earlier_t, -5000.0)
+    peers = [(n, twin_bit) for n in range(chips) for twin_bit in range(2)][1:]
+    place_copies = {
+        (n, b): remote(place_all.at[0, 0], place_all.at[n, b], (flip(me, 2 * n + b), t)) for n, b in peers
+    }
 
     loads[0].wait()
     for copy in gather0:
@@ -384,9 +374,24 @@
     pre = readout + skip_ref[...] * mix_f
     mixer = 0.5 * pre * (1.0 + erf(pre * 0.7071067811865476))
     mix_all[t] = mixer.astype(bf16)
-    gather1 = [tp_copy(1, k, mix_all.at[t], mix_all.at[t]) for k in range(1, tp)]
-    for copy in gather1:
-        copy.start()
+    gather1 = gather(mix_all.at[t], mix_all.at[t])
+
+    for copy in place_copies.values():
+        copy.wait_recv()
+    iota_r = lax.broadcasted_iota(jnp.int32, (rows, seqs), 0).astype(f32)
+    iota_l = lax.broadcasted_iota(jnp.int32, (seqs, rows), 1).astype(f32)
+
+    def slot_row(n, b):
+        return place_all[n, b, pl.ds(me, 1), 0:seqs] + float((n % 2 * 2 + b) * cap)
+
+    for n in range(chips):
+        for b in range(2):
+            slots = slot_row(n, b)
+            span = slice((n % 2 * 2 + b) * seqs, (n % 2 * 2 + b + 1) * seqs)
+            pick[n // 2, :, span] = jnp.where(iota_r == slots, 1.0, 0.0).astype(bf16)
+            down = jnp.sum(jnp.where(row_i == col_i, slots, 0.0), axis=1, keepdims=True)
+            spill[n, b * seqs : (b + 1) * seqs, :] = jnp.where(iota_l == down, 1.0, 0.0).astype(bf16)
+
     loads[3].wait()
     for copy in gather1:
         copy.wait_recv()
@@ -394,9 +399,7 @@
     for j in range(tp):
         glu_gate = glu_gate + dot(mix_all[j], glu[j * chans : (j + 1) * chans, :])
     gated_all[t] = (mixer * jax.nn.sigmoid(glu_gate)).astype(bf16)
-    gather2 = [tp_copy(2, k, gated_all.at[t], gated_all.at[t]) for k in range(1, tp)]
-    for copy in gather2:
-        copy.start()
+    gather2 = gather(gated_all.at[t], gated_all.at[t])
     loads[4].wait()
     for copy in gather2:
         copy.wait_recv()
@@ -406,136 +409,182 @@
     stream = mixed.astype(bf16)
     stream_f = stream.astype(f32)
 
-    iota_p = lax.broadcasted_iota(jnp.int32, (ep, packed, seqs), 1).astype(f32)
-    place_b = jnp.broadcast_to(place_t[:, None, :], (ep, packed, seqs))
-    tokens = jnp.zeros((items, 128), f32)
-    for c in range(chunks):
-        choose = jnp.where(iota_p - c * cap == place_b, 1.0, 0.0)
-        tokens = tokens + dot(
-            choose.astype(bf16).reshape(items, seqs), stream[:, c * 128 : (c + 1) * 128]
+    def place_of(n, b):
+        return pl.ds((n % 2) * pair + b * seqs, seqs)
+
+    tok[0, t, 0:seqs, :] = stream
+    here = {}
+    twin_in = {}
+
+    def slab(n, j, b=0, cut=None):
+        begin, size = (n % 2) * pair + b * seqs, seqs
+        if cut is not None:
+            begin, size = begin + cut * half, half
+        return tok.at[n // 2, j, pl.ds(begin, size)]
+
+    def to_twin(n, key, j, cut=None):
+        twin_in[n, key] = remote(slab(n, j, 0, cut), slab(n, j, 1, cut), twin)
+
+    def spread_chips():
+        for n in range(1, chips):
+            here[n, "z"] = remote(slab(0, t), slab(n, t), (flip(me, 2 * n), t))
+
+    def enter(n):
+        if n:
+            here[n, "z"].wait_recv()
+        here[n, "b"] = remote(slab(n, t), slab(n, t), side_b)
+        here[n, "a"] = remote(slab(n, t), slab(n, t), side_a)
+        to_twin(n, "t", t)
+
+    def relay(n):
+        here[n, "b"].wait_recv()
+        here[n, "ob"] = remote(slab(n, beside, 0, 0), slab(n, beside, 0, 0), side_a)
+        to_twin(n, "b", beside)
+        here[n, "a"].wait_recv()
+        here[n, "oa"] = remote(slab(n, across, 0, 1), slab(n, across, 0, 1), side_b)
+        to_twin(n, "a", across)
+
+    def corner(n):
+        here[n, "ob"].wait_recv()
+        to_twin(n, "o0", opposite, 0)
+        here[n, "oa"].wait_recv()
+        to_twin(n, "o1", opposite, 1)
+
+    def logits():
+        logit_all[t] = jnp.zeros(logit_all.shape[1:], f32)
+        logit_all[t, 0:ep, 0:seqs] = lax.dot_general(
+            router_ref[:, pl.ds(pl.multiple_of(t * cols, cols), cols)],
+            stream_f * gain2_ref[t],
+            last,
+            precision=lax.Precision.HIGHEST,
+            preferred_element_type=f32,
         )
-    buf[...] = tokens.astype(bf16).reshape(ep, packed, 128)
-    sends = [ep_copy(0, k, buf.at[(me + k) % ep], recv.at[me]) for k in range(1, ep)]
-    for copy in sends:
-        copy.start()
-    recv[me] = buf[me]
-
-    logit_all[t] = jnp.zeros(logit_all.shape[1:], f32)
-    logit_all[t, :, 0:ep] = lax.dot_general(
-        stream_f * gain2_ref[t],
-        router_ref[:, pl.ds(pl.multiple_of(t * cols, cols), cols)],
-        last,
-        precision=lax.Precision.HIGHEST,
-        preferred_element_type=f32,
-    )
-    logit_all[t, :, ep : ep + 1] = jnp.sum(stream_f * stream_f, axis=1, keepdims=True)
-    gather3 = [tp_copy(3, k, logit_all.at[t], logit_all.at[t]) for k in range(1, tp)]
-    for copy in gather3:
-        copy.start()
-
-    for copy in sends:
-        copy.wait_recv()
-    received = recv[...].reshape(items, 128)
-    for c in range(chunks):
-        tok_all[t, :, c * 128 : (c + 1) * 128] = dot(unpack[c], received).astype(bf16)
-    beside, across = t + 1 - 2 * (t % 2), (t + 2) % tp
-    opposite = (beside + 2) % tp
-    half = rows // 32 * 16
-
-    def side_copy(phase, n, block, peer):
-        return pltpu.make_async_remote_copy(
-            src_ref=block,
-            dst_ref=block,
-            send_sem=tp_send.at[phase, n],
-            recv_sem=tp_recv.at[phase, n],
-            device_id=(me, peer),
-            device_id_type=pl.DeviceIdType.MESH,
+        energy = jnp.sum(stream_f * stream_f, axis=1, keepdims=True)
+        logit_all[t, ep : ep + 1, 0:seqs] = jnp.sum(
+            jnp.where(row_i == col_i, energy, 0.0), axis=0, keepdims=True
         )
-
-    gather4 = [
-        side_copy(4, 0, tok_all.at[t], beside),
-        side_copy(4, 1, tok_all.at[t], across),
-        side_copy(4, 2, tok_all.at[beside, pl.ds(0, half)], across),
-        side_copy(4, 3, tok_all.at[across, pl.ds(half, rows - half)], beside),
-    ]
-    gather4[0].start()
-    gather4[1].start()
-
-    for copy in gather3:
-        copy.wait_recv()
-    summed = logit_all[0]
-    for j in range(1, tp):
-        summed = summed + logit_all[j]
-    inverse = lax.rsqrt(summed[:, ep : ep + 1] / width + EPSILON)
-    logits = summed[:, 0:ep] * inverse
-    chosen = routed > 0.5
-    expon = jnp.where(chosen, jnp.exp(jnp.where(chosen, logits, 0.0)), 0.0)
-    weights = expon / jnp.sum(expon, axis=1, keepdims=True)
-
-    loads[5].wait()
-    loads[6].wait()
-    squares = jnp.zeros((rows, 1), f32)
-    for n, j in enumerate([t, beside, across, opposite]):
-        if n == 1:
-            gather4[0].wait_recv()
-            gather4[2].start()
-            gather4[1].wait_recv()
-            gather4[3].start()
-        if n == 3:
-            gather4[2].wait_recv()
-            gather4[3].wait_recv()
-        part = tok_all[j].astype(f32)
-        squares = squares + jnp.sum(part * part, axis=1, keepdims=True)
+        here["logits"] = gather(logit_all.at[t], logit_all.at[t])
+
+    def weights():
+        for copy in here["logits"]:
+            copy.wait_recv()
+        whole = logit_all[0]
+        for j in range(1, tp):
+            whole = whole + logit_all[j]
+        whole = whole[:, 0:seqs]
+        inverse = lax.rsqrt(whole[ep : ep + 1] / width + EPSILON)
+        chosen = routed_t > 0.5
+        expon = jnp.where(chosen, jnp.exp(jnp.where(chosen, whole[0:ep] * inverse, 0.0)), 0.0)
+        weight_all[0, 0] = jnp.zeros(weight_all.shape[2:], f32)
+        weight_all[0, 0, 0:ep, 0:seqs] = expon / jnp.sum(expon, axis=0, keepdims=True)
+        weight_all[0, 0, ep : ep + 1, 0:seqs] = inverse
+        for n, b in peers:
+            here["w", n, b] = remote(weight_all.at[0, 0], weight_all.at[n, b], (flip(me, 2 * n + b), t))
+
+    def expert_in(h, block):
+        j = {"t": t, "b": beside, "a": across, "o": opposite}[block]
+        if (h, block) == (0, "t"):
+            loads[5].wait()
+            loads[6].wait()
+        for n in (2 * h, 2 * h + 1):
+            for key in ("o0", "o1") if block == "o" else (block,):
+                twin_in[n, key].wait_recv()
+        part = dot(pick[h], tok[h, j])
         scaled = (part * gain2_ref[j]).astype(bf16)
         span = pl.ds(pl.multiple_of(j * cols, cols), cols)
-        if n == 0:
+        if block == "t":
             acc_g[...] = dot(scaled, wg[span, :])
             acc_u[...] = dot(scaled, wu[span, :])
         else:
             acc_g[...] += dot(scaled, wg[span, :])
             acc_u[...] += dot(scaled, wu[span, :])
-    norm = lax.rsqrt(squares / width + EPSILON)
-    gate_cl = jnp.minimum(acc_g[...] * norm, LIMIT)
-    up_cl = jnp.clip(acc_u[...] * norm, -LIMIT, LIMIT)
-    active = ((up_cl + 1.0) * (gate_cl * jax.nn.sigmoid(ALPHA * gate_cl))).astype(bf16)
-    for load in loads[7:]:
-        load.wait()
-    scatter = {k: tp_copy(5, k, part_out.at[k], part_in.at[k]) for k in range(1, tp)}
-    for k in order:
-        part_out[k] = dot(active, wd[(t + k) % tp]).astype(bf16)
-        scatter[k].start()
-    result = dot(active, wd[t]).astype(bf16).astype(f32)
-
-    expand = jnp.where(lax.broadcasted_iota(jnp.int32, (ep, items), 0) == owner, 1.0, 0.0).astype(bf16)
-    place_x = dot(place.astype(bf16), expand)
-    weight_x = dot(weights.astype(bf16), expand)
-    within_f = within.astype(f32)
-    combine = [
-        jnp.where(within_f - c * cap == place_x, weight_x, 0.0).astype(bf16) for c in range(chunks)
+
+    def activate(h):
+        norm = jnp.zeros((rows, 1), f32)
+        share = jnp.zeros((rows, 1), f32)
+        for n in (2 * h, 2 * h + 1):
+            for b in range(2):
+                if (n, b) != (0, 0):
+                    here["w", n, b].wait_recv()
+                match = iota_r == slot_row(n, b)
+                inverse = weight_all[n, b, ep : ep + 1, 0:seqs]
+                weight = weight_all[n, b, pl.ds(me, 1), 0:seqs]
+                norm = norm + jnp.sum(jnp.where(match, inverse, 0.0), axis=1, keepdims=True)
+                share = share + jnp.sum(jnp.where(match, weight, 0.0), axis=1, keepdims=True)
+        gate_cl = jnp.minimum(acc_g[...] * norm, LIMIT)
+        up_cl = jnp.clip(acc_u[...] * norm, -LIMIT, LIMIT)
+        act[h] = (((up_cl + 1.0) * share) * (gate_cl * jax.nn.sigmoid(ALPHA * gate_cl))).astype(bf16)
+
+    def expert_out(n):
+        if n == firsts[0]:
+            for load in loads[7:]:
+                load.wait()
+        spread_act = dot(spill[n], act[n // 2]).astype(bf16)
+        for key, j in (("o", opposite), ("b", beside), ("a", across), ("t", t)):
+            value = dot(spread_act, wd[j])
+            sib_out[n, j] = value[seqs:].astype(bf16)
+            here[n, "s" + key] = remote(sib_out.at[n, j], sib_in.at[n, j], twin)
+            mine[n, j] = value[:seqs]
+
+    def reduce_chip(n):
+        here[n, "so"].wait_recv()
+        summed[n, opposite] = (mine[n, opposite] + sib_in[n, opposite].astype(f32)).astype(bf16)
+        top, bottom = pl.ds(0, half), pl.ds(half, half)
+        here[n, "fb"] = remote(summed.at[n, opposite, top], fwd_in.at[n, 0], side_b)
+        here[n, "fa"] = remote(summed.at[n, opposite, bottom], fwd_in.at[n, 1], side_a)
+        here[n, "sb"].wait_recv()
+        both = mine[n, beside] + sib_in[n, beside].astype(f32)
+        mine[n, beside] = both
+        summed[n, beside, 0:half] = both[0:half].astype(bf16)
+        here[n, "db"] = remote(summed.at[n, beside, top], from_side.at[n, 0, top], side_b)
+        here[n, "sa"].wait_recv()
+        both = mine[n, across] + sib_in[n, across].astype(f32)
+        mine[n, across] = both
+        summed[n, across, half:] = both[half:].astype(bf16)
+        here[n, "da"] = remote(summed.at[n, across, bottom], from_side.at[n, 1, bottom], side_a)
+
+    def reduce_relay(n):
+        top, bottom = pl.ds(0, half), pl.ds(half, half)
+        here[n, "fb"].wait_recv()
+        fwd_out[n, 0] = (mine[n, across, 0:half] + fwd_in[n, 0].astype(f32)).astype(bf16)
+        here[n, "ga"] = remote(fwd_out.at[n, 0], from_side.at[n, 1, top], side_a)
+        here[n, "fa"].wait_recv()
+        fwd_out[n, 1] = (mine[n, beside, half:] + fwd_in[n, 1].astype(f32)).astype(bf16)
+        here[n, "gb"] = remote(fwd_out.at[n, 1], from_side.at[n, 0, bottom], side_b)
+
+    def go_home(n):
+        here[n, "st"].wait_recv()
+        value = mine[n, t] + sib_in[n, t].astype(f32)
+        for key in ("db", "da", "ga", "gb"):
+            here[n, key].wait_recv()
+        value = value + from_side[n, 0].astype(f32) + from_side[n, 1].astype(f32)
+        if n:
+            home_out[n] = value.astype(bf16)
+            here[n, "h"] = remote(home_out.at[n], home_in.at[n], (flip(me, 2 * n), t))
+        else:
+            mine[n, t] = value
+
+    def finish():
+        result = stream_f + mine[0, t]
+        for n in range(1, chips):
+            here[n, "h"].wait_recv()
+            result = result + home_in[n].astype(f32)
+        out_ref[...] = result.astype(bf16)
+
+    firsts = (1,)
+    plan = [
+        (spread_chips,), (enter, 0), (logits,),
+        (enter, 1), (relay, 0), (weights,), (corner, 0), (enter, 2), (relay, 1),
+        (expert_in, 0, "t"), (enter, 3), (corner, 1), (expert_in, 0, "b"), (relay, 2), (expert_in, 0, "a"),
+        (expert_in, 0, "o"), (corner, 2), (relay, 3), (activate, 0), (expert_out, 1), (corner, 3), (expert_out, 0),
+        (reduce_chip, 1), (expert_in, 1, "t"), (reduce_chip, 0), (expert_in, 1, "b"), (reduce_relay, 1), (expert_in, 1, "a"),
+        (reduce_relay, 0), (expert_in, 1, "o"), (activate, 1), (expert_out, 3), (go_home, 1), (expert_out, 2),
+        (go_home, 0), (reduce_chip, 3), (reduce_chip, 2), (reduce_relay, 3), (reduce_relay, 2), (go_home, 3), (go_home, 2),
+        (finish,),
     ]
-    for k in order:
-        scatter[k].wait_recv()
-        result = result + part_in[k].astype(f32)
-    result = result.astype(bf16)
-    outgoing = jnp.zeros((items, 128), f32)
-    for c in range(chunks):
-        outgoing = outgoing + dot(repack[c], result[:, c * 128 : (c + 1) * 128])
-    back[...] = outgoing.astype(bf16).reshape(ep, packed, 128)
-    returns = [ep_copy(1, k, back.at[(me + k) % ep], fin.at[me]) for k in range(1, ep)]
-    for copy in returns:
-        copy.start()
-    fin[me] = back[me]
-    for copy in returns:
-        copy.wait_recv()
-    final = fin[...].reshape(items, 128)
-    for c in range(chunks):
-        span = slice(c * 128, (c + 1) * 128)
-        out_ref[:, span] = (stream_f[:, span] + dot(combine[c], final)).astype(bf16)
-    for copy in gather0 + gather1 + gather2 + gather3 + sends + returns:
-        copy.wait_send()
-    for k in order:
-        scatter[k].wait_send()
-    for copy in gather4:
+    for step in plan:
+        step[0](*step[1:])
+    for copy in copies:
         copy.wait_send()
     for store in stores:
         store.wait()
@@ -569,19 +618,21 @@
     seqs, cols = residual.shape
     groups, states = decay_rate.shape
     chans = skip_gain.shape[0]
-    if gate_weight.shape[0] != 1 or groups % 16 or chans % 128 or cols % 128 or tp != 4 or seqs % 16:
+    rough = groups % 16 or chans % 128 or cols % 128 or seqs % 32 or seqs > 128
+    if gate_weight.shape[0] != 1 or tp != 4 or ep != 8 or rough:
         return per_device(*args)
     top = route_ids.shape[1]
     cap = seqs * top // router.shape[1] + 1
-    packed = -(-cap * (cols // 128) // 16) * 16
-    rows = -(-ep * cap // 16) * 16
+    rows = -(-4 * cap // 16) * 16
     hidden = gate_weight.shape[2]
-    items = ep * packed
+    chips = ep // 2
+    halves = chips // 2
     bf16, f32 = jnp.bfloat16, jnp.float32
     vmem, anywhere = pl.BlockSpec(memory_space=pltpu.VMEM), pl.BlockSpec(memory_space=pl.ANY)
     state_shape = (seqs, groups, states)
+    blocks = (chips, tp, seqs, cols)
     out = pl.pallas_call(
-        functools.partial(layer_kernel, (ep, tp, cap, packed, rows)),
+        functools.partial(layer_kernel, (ep, tp, cap, rows)),
         out_shape=(
             jax.ShapeDtypeStruct((seqs, cols), bf16),
             jax.ShapeDtypeStruct(state_shape, f32),
@@ -601,24 +652,28 @@
             pltpu.VMEM((tp, seqs, cols), bf16),
             pltpu.VMEM((tp, seqs, chans), bf16),
             pltpu.VMEM((tp, seqs, chans), bf16),
-            pltpu.VMEM((tp, seqs, 128), f32),
-            pltpu.VMEM((ep, packed, 128), bf16),
-            pltpu.VMEM((ep, packed, 128), bf16),
-            pltpu.VMEM((tp, rows, cols), bf16),
+            pltpu.VMEM((tp, 2 * ep, 128), f32),
+            pltpu.VMEM((chips, 2, ep, 128), f32),
+            pltpu.VMEM((chips, 2, 2 * ep, 128), f32),
+            pltpu.VMEM((halves, rows, 4 * seqs), bf16),
+            pltpu.VMEM((chips, 2 * seqs, rows), bf16),
+            pltpu.VMEM((halves, tp, 4 * seqs, cols), bf16),
             pltpu.VMEM((rows, hidden), f32),
             pltpu.VMEM((rows, hidden), f32),
-            pltpu.VMEM((tp, rows, cols), bf16),
-            pltpu.VMEM((tp, rows, cols), bf16),
-            pltpu.VMEM((cols // 128, rows, items), bf16),
-            pltpu.VMEM((cols // 128, items, rows), bf16),
-            pltpu.VMEM((ep, packed, 128), bf16),
-            pltpu.VMEM((ep, packed, 128), bf16),
+            pltpu.VMEM((halves, rows, hidden), bf16),
+            pltpu.VMEM(blocks, f32),
+            pltpu.VMEM(blocks, bf16),
+            pltpu.VMEM(blocks, bf16),
+            pltpu.VMEM(blocks, bf16),
+            pltpu.VMEM((chips, 2, seqs, cols), bf16),
+            pltpu.VMEM((chips, 2, seqs // 2, cols), bf16),
+            pltpu.VMEM((chips, 2, seqs // 2, cols), bf16),
+            pltpu.VMEM((chips, seqs, cols), bf16),
+            pltpu.VMEM((chips, seqs, cols), bf16),
             pltpu.SemaphoreType.DMA((7 + tp,)),
             pltpu.SemaphoreType.DMA((2,)),
-            pltpu.SemaphoreType.DMA((6, tp)),
-            pltpu.SemaphoreType.DMA((6, tp)),
-            pltpu.SemaphoreType.DMA((2, ep)),
-            pltpu.SemaphoreType.DMA((2, ep)),
+            pltpu.SemaphoreType.DMA((128,)),
+            pltpu.SemaphoreType.DMA((128,)),
         ],
         compiler_params=pltpu.CompilerParams(
             collective_id=0, has_side_effects=True, vmem_limit_bytes=60 * 1024 * 1024

time: 67.4 us -> 66.4 us (0.985)
  Pallas kernels: 66.6 us -> 65.6 us
    pallas_call x1, Pallas kernels: 64.5 us -> 63.5 us  [dispatch(): pl.pallas_call(functools.partial(layer_kernel, (ep, tp, cap, rows)), out_...]
where the time goes in v1:
time: 66.4 us; the launch traced here: 66.2 us
  Pallas kernels  65.6 us (99%)
    pallas_call x1, Pallas kernels, dispatch(): pl.pallas_call(functools.partial(layer_kernel, (ep, tp, cap, rows)), out_...  63.5 us
    pallas_call x1, Pallas kernels, dispatch(): pl.pallas_call(finish_kernel, out_shape=tuple((jax.ShapeDtypeStruct(part....  2.1 us

profile of v1, /device:TPU:0, one launch (start us, length us, event | category | flops | bytes accessed | tf_op | source)
XLA Modules:
  0.0 66.2 jit_solution(17641274294110715058)
XLA Ops:
  0.6 63.5 %layer.1 = (bf16[64,512]{1,0:T(8,128)(2,1)}, f32[64,16,64]{2,1,0:T(8,128)}, f32[64,16,64]{2,1,0:T(8,128)}) custom-call(bf16[64,512]{1,0:T(8,128)(2,1)} %resid_ref.1, f32[4,1,512]{2,1,0:T(1,128)} %bitcast.21, f32[16,64]{1,0:T(8,128)} %decay_ref.1, f32[16,64]{1,0:T(8,128)} %freq_ref.1, f32[1,16]{1,0:T(1,128)} %bitcast.25, f32[16,16,64]{2,1,0:T(8,128)} %bitcast.16, ...), custom_call_target="tpu_custom_call" | custom-call | tf_op jit(solution)/shard_map/layer/pallas_call | solution.py:634
  64.1 2.1 %finish.1 = (bf16[64,512]{1,0:T(8,128)(2,1)}, f32[64,16,64]{2,1,0:T(8,128)}, f32[64,16,64]{2,1,0:T(8,128)}) custom-call(bf16[64,512]{1,0:T(8,128)(2,1)} %get-tuple-element.6.a_in, f32[64,16,64]{2,1,0:T(8,128)} %get-tuple-element.7.b_in, f32[64,16,64]{2,1,0:T(8,128)} %get-tuple-element.8.c_in), custom_call_target="tpu_custom_call" | custom-call | tf_op jit(solution)/shard_map/finish/pallas_call | solution.py:705

commit v2 on v1

v2 whole, which is shorter than its diff:
```python
import functools

import jax
import jax.numpy as jnp
from jax import lax
from jax.experimental import pallas as pl
from jax.experimental.pallas import tpu as pltpu
from jax.sharding import PartitionSpec as P

EPSILON = 1e-05
LIMIT = 7.0
ALPHA = 1.702


def discretise(decay_rate, frequency, log_step, input_re, input_im):
    real_part = -decay_rate
    step_size = jnp.exp(log_step)[:, None]
    magnitude = jnp.exp(step_size * real_part)
    abar_re = magnitude * jnp.cos(step_size * frequency)
    abar_im = magnitude * jnp.sin(step_size * frequency)
    denom = real_part * real_part + frequency * frequency
    minus_one = abar_re - 1.0
    coef_re = (minus_one * real_part + abar_im * frequency) / denom
    coef_im = (abar_im * real_part - minus_one * frequency) / denom
    bbar_re = coef_re[..., None] * input_re - coef_im[..., None] * input_im
    bbar_im = coef_re[..., None] * input_im + coef_im[..., None] * input_re
    return (abar_re, abar_im, bbar_re, bbar_im)


def per_device(
    residual,
    state_re,
    state_im,
    mix_gain,
    proj_in,
    decay_rate,
    frequency,
    log_step,
    input_re,
    input_im,
    read_re,
    read_im,
    skip_gain,
    glu_weight,
    out_proj,
    ffn_gain,
    router,
    gate_weight,
    up_weight,
    down_weight,
    route_ids,
):
    high = lax.Precision.HIGHEST
    seq_rows = residual.shape[0]
    col_count = residual.shape[1]
    width = mix_gain.shape[0]
    ep_size = lax.axis_size("ep")
    own_resid = residual.astype(jnp.float32)
    full_resid = lax.all_gather(residual, "tp", axis=1, tiled=True).astype(jnp.float32)
    scale_one = lax.rsqrt(jnp.mean(full_resid * full_resid, axis=1, keepdims=True) + EPSILON)
    xnorm = (full_resid * scale_one * mix_gain).astype(jnp.bfloat16)
    mix_in = jnp.dot(xnorm, proj_in, preferred_element_type=jnp.float32).astype(jnp.bfloat16)
    mix_f = mix_in.astype(jnp.float32)
    group_count = decay_rate.shape[0]
    group_width = input_re.shape[2]
    grouped = mix_f.reshape(seq_rows, group_count, group_width)
    abar_re, abar_im, bbar_re, bbar_im = discretise(
        decay_rate, frequency, log_step, input_re, input_im
    )
    drive_re = jnp.einsum("sgc,gnc->sgn", grouped, bbar_re, precision=high)
    drive_im = jnp.einsum("sgc,gnc->sgn", grouped, bbar_im, precision=high)
    state_re_new = abar_re * state_re - abar_im * state_im + drive_re
    state_im_new = abar_re * state_im + abar_im * state_re + drive_im
    readout = jnp.einsum("sgn,gcn->sgc", state_re_new, read_re, precision=high) - jnp.einsum(
        "sgn,gcn->sgc", state_im_new, read_im, precision=high
    )
    mixer = jax.nn.gelu(
        readout.reshape(seq_rows, group_count * group_width) + skip_gain * mix_f, approximate=False
    )
    all_mixer = lax.all_gather(mixer.astype(jnp.bfloat16), "tp", axis=1, tiled=True)
    glu_gate = jnp.dot(all_mixer, glu_weight, preferred_element_type=jnp.float32)
    gated = (mixer * jax.nn.sigmoid(glu_gate)).astype(jnp.bfloat16)
    all_gated = lax.all_gather(gated, "tp", axis=1, tiled=True)
    mixed = jnp.dot(all_gated, out_proj, preferred_element_type=jnp.float32)
    stream = (own_resid + mixed).astype(jnp.bfloat16)
    stream_f = stream.astype(jnp.float32)
    all_stream = lax.all_gather(stream, "tp", axis=1, tiled=True).astype(jnp.float32)
    inverse = lax.rsqrt(jnp.mean(all_stream * all_stream, axis=1, keepdims=True) + EPSILON)
    logits = jnp.dot(all_stream * ffn_gain, router, precision=high) * inverse
    payload = (all_stream * inverse * ffn_gain).astype(jnp.bfloat16)
    expert_count = router.shape[1]
    top_count = route_ids.shape[1]
    capacity = seq_rows * top_count // expert_count + 1
    expert_iota = jnp.arange(expert_count, dtype=jnp.int32)
    choose = (route_ids[:, :, None] == expert_iota).astype(jnp.float32)
    picked = jnp.sum(choose * logits[:, None, :], axis=2)
    expon = jnp.exp(picked)
    weights = expon / jnp.sum(expon, axis=1, keepdims=True)
    flat_route = route_ids.reshape(seq_rows * top_count)
    one_hot = (flat_route[:, None] == expert_iota).astype(jnp.int32)
    before = jnp.cumsum(one_hot, axis=0) - one_hot
    slot_ids = jnp.sum(before * one_hot, axis=1)
    target = flat_route * capacity + slot_ids
    slot_iota = jnp.arange(expert_count * capacity, dtype=jnp.int32)
    placing = jnp.any(slot_iota[:, None, None] == target.reshape(seq_rows, top_count)[None], axis=2)
    buffer = jnp.dot(placing.astype(jnp.bfloat16), payload, preferred_element_type=jnp.float32)
    buffer = buffer.astype(jnp.bfloat16).reshape(expert_count, capacity, payload.shape[1])
    local_experts = gate_weight.shape[0]
    received = lax.all_to_all(buffer, "ep", split_axis=0, concat_axis=0, tiled=True)
    items = received.shape[1]
    tokens = received.reshape(ep_size, local_experts, items, width)
    tokens = tokens.transpose(1, 0, 2, 3).reshape(local_experts, ep_size * items, width)
    gate_pre = jnp.einsum("esd,edf->esf", tokens, gate_weight, preferred_element_type=jnp.float32)
    up_pre = jnp.einsum("esd,edf->esf", tokens, up_weight, preferred_element_type=jnp.float32)
    gate_cl = jnp.minimum(gate_pre, LIMIT)
    up_cl = jnp.clip(up_pre, -LIMIT, LIMIT)
    active = ((up_cl + 1.0) * (gate_cl * jax.nn.sigmoid(ALPHA * gate_cl))).astype(jnp.bfloat16)
    partial_value = jnp.einsum(
        "esf,efd->esd", active, down_weight, preferred_element_type=jnp.float32
    ).astype(jnp.bfloat16)
    summed = lax.psum_scatter(
        partial_value.astype(jnp.float32).astype(jnp.bfloat16),
        "tp",
        scatter_dimension=2,
        tiled=True,
    )
    outgoing = summed.reshape(local_experts, ep_size, items, col_count)
    outgoing = outgoing.transpose(1, 0, 2, 3).reshape(ep_size * local_experts, items, col_count)
    returned = lax.all_to_all(outgoing, "ep", split_axis=0, concat_axis=0, tiled=True)
    flat_back = returned.reshape(expert_count * capacity, col_count)
    fetched = (
        jnp.take(flat_back, target, axis=0)
        .astype(jnp.float32)
        .reshape(seq_rows, top_count, col_count)
    )
    experts_sum = jnp.sum(weights[..., None] * fetched, axis=1)
    layer_out = (stream_f + experts_sum).astype(jnp.bfloat16)
    return (layer_out, state_re_new, state_im_new)


def erf(x):
    x = jnp.clip(x, -3.832506856900711, 3.832506856900711)
    y = x * x
    top = 0.00022905065861350646
    for coefficient in (
        0.0034082910107109506,
        0.050955695062380861,
        0.18520832239976145,
        1.128379143519084,
    ):
        top = top * y + coefficient
    bottom = -1.1791602954361697e-7
    for coefficient in (
        0.000023547966471313185,
        0.0010179625278914885,
        0.014070470171167667,
        0.11098505178285362,
        0.49746925110067538,
        1.0,
    ):
        bottom = bottom * y + coefficient
    return x * top / bottom


SENDS = ("g0", "g1", "g2", "g3", "place", "weight", "chips", "side", "relay", "twin", "back", "sum", "home")


def layer_kernel(
    sizes,
    resid_hbm,
    gain1_hbm,
    gain2_hbm,
    decay_hbm,
    freq_hbm,
    step_hbm,
    in_re_hbm,
    in_im_hbm,
    read_re_hbm,
    read_im_hbm,
    skip_hbm,
    router_hbm,
    route_hbm,
    sre_hbm,
    sim_hbm,
    proj_hbm,
    glu_hbm,
    outp_hbm,
    gate_hbm,
    up_hbm,
    down_hbm,
    out_ref,
    sre_out,
    sim_out,
    resid_ref,
    gains,
    poles,
    step_ref,
    in_maps,
    read_maps,
    skip_ref,
    router_ref,
    route_ref,
    state,
    proj,
    glu,
    outp,
    wg,
    wu,
    wd,
    res_all,
    mix_all,
    gated_all,
    logit_all,
    place_all,
    weight_all,
    pick,
    spill,
    tok,
    acc_g,
    acc_u,
    act,
    mine,
    sib_out,
    sib_in,
    summed,
    from_side,
    fwd_in,
    fwd_out,
    home_out,
    home_in,
    load_sem,
    send_sem,
    recv_sem,
):
    ep, tp, cap, rows = sizes
    f32, bf16 = jnp.float32, jnp.bfloat16
    me, t = lax.axis_index("ep"), lax.axis_index("tp")
    seqs, cols = resid_ref.shape
    width = cols * tp
    _, groups, states = poles.shape
    chans = skip_ref.shape[1]
    group_width = chans // groups
    chips = ep // 2
    pair = 2 * seqs
    half = seqs // 2
    last = (((1,), (1,)), ((), ()))

    def dot(a, b):
        return jnp.dot(a, b, preferred_element_type=f32)

    batches = {
        "resid": (resid_ref, [(resid_hbm, resid_ref)]),
        "route": (route_ref, [(route_hbm, route_ref)]),
        "step": (step_ref, [(step_hbm, step_ref)]),
        "poles": (poles, [(decay_hbm, poles.at[0]), (freq_hbm, poles.at[1])]),
        "in": (in_maps, [(in_re_hbm, in_maps.at[0]), (in_im_hbm, in_maps.at[1])]),
        "gains": (gains, [(gain1_hbm, gains.at[0]), (gain2_hbm, gains.at[1])]),
        "proj": (proj, [(proj_hbm, proj)]),
        "state": (state, [(sre_hbm, state.at[0]), (sim_hbm, state.at[1])]),
        "read": (read_maps, [(read_re_hbm, read_maps.at[0]), (read_im_hbm, read_maps.at[1])]),
        "skip": (skip_ref, [(skip_hbm, skip_ref)]),
        "glu": (glu, [(glu_hbm, glu)]),
        "outp": (outp, [(outp_hbm, outp)]),
        "router": (router_ref, [(router_hbm, router_ref)]),
        "gate": (wg, [(gate_hbm, wg)]),
        "up": (wu, [(up_hbm, wu)]),
        "down": (wd, [(down_hbm.at[:, j * cols : (j + 1) * cols], wd.at[j]) for j in range(tp)]),
    }
    names = list(batches)

    def absorb(ref, sem):
        pltpu.make_async_copy(ref, ref, sem).wait()

    def loaded(*wanted):
        for name in wanted:
            absorb(batches[name][0], load_sem.at[names.index(name)])

    for n, name in enumerate(names):
        for source, held in batches[name][1]:
            pltpu.make_async_copy(source, held, load_sem.at[n]).start()

    barrier = pltpu.get_barrier_semaphore()
    for k in range(1, tp):
        pl.semaphore_signal(barrier, inc=1, device_id=(me, (t + k) % tp), device_id_type=pl.DeviceIdType.MESH)
    for k in range(1, ep):
        pl.semaphore_signal(barrier, inc=1, device_id=((me + k) % ep, t), device_id_type=pl.DeviceIdType.MESH)
    pl.semaphore_wait(barrier, tp + ep - 2)

    arrivals = []

    def arrival(key):
        if key not in arrivals:
            arrivals.append(key)
        return recv_sem.at[arrivals.index(key)]

    def remote(source, target, peer, kind, key):
        pltpu.make_async_remote_copy(
            src_ref=source,
            dst_ref=target,
            send_sem=send_sem.at[SENDS.index(kind)],
            recv_sem=arrival(key),
            device_id=peer,
            device_id_type=pl.DeviceIdType.MESH,
        ).start()

    def flip(value, k):
        for bit in (1, 2, 4, 8, 16):
            if k & bit:
                value = value + bit - 2 * bit * ((value // bit) % 2)
        return value

    beside, across = flip(t, 1), flip(t, 2)
    opposite = flip(beside, 2)
    sibling = flip(me, 1)
    side_b, side_a, side_o, twin = (me, beside), (me, across), (me, opposite), (sibling, t)

    def gather(source, target, name):
        for k in (3, 1, 2):
            remote(source, target, (me, flip(t, k)), name, name)

    loaded("resid")
    gather(resid_ref, res_all.at[t], "g0")
    res_all[t] = resid_ref[...]

    loaded("route", "step", "poles", "in")
    square = (groups, groups)
    diagonal = lax.broadcasted_iota(jnp.int32, square, 0) == lax.broadcasted_iota(jnp.int32, square, 1)
    log_step = jnp.sum(
        jnp.where(diagonal, jnp.broadcast_to(step_ref[...], square), 0.0), axis=1, keepdims=True
    )
    step_size = jnp.exp(log_step)
    real_part, imag_part = -poles[0], poles[1]
    magnitude = jnp.exp(step_size * real_part)
    abar_re = magnitude * jnp.cos(step_size * imag_part)
    abar_im = magnitude * jnp.sin(step_size * imag_part)
    denom = real_part * real_part + imag_part * imag_part
    minus_one = abar_re - 1.0
    coef_re = ((minus_one * real_part + abar_im * imag_part) / denom)[:, None, :]
    coef_im = ((abar_im * real_part - minus_one * imag_part) / denom)[:, None, :]
    in_re, in_im = in_maps[0], in_maps[1]
    bb_re = (coef_re * in_re - coef_im * in_im).astype(bf16).reshape(chans, states)
    bb_im = (coef_re * in_im + coef_im * in_re).astype(bf16).reshape(chans, states)
    abar_re, abar_im = abar_re[None], abar_im[None]

    route = route_ref[...]
    iota_e = lax.broadcasted_iota(jnp.int32, (ep, seqs), 0)
    routed_t = jnp.zeros((ep, seqs), f32)
    for j in range(route.shape[0]):
        routed_t = routed_t + jnp.where(route[j : j + 1, :] == iota_e, 1.0, 0.0)
    row_i = lax.broadcasted_iota(jnp.int32, (seqs, seqs), 0)
    col_i = lax.broadcasted_iota(jnp.int32, (seqs, seqs), 1)
    earlier_t = dot(routed_t.astype(bf16), jnp.where(row_i < col_i, 1.0, 0.0).astype(bf16))
    place_all[0] = jnp.zeros(place_all.shape[1:], f32)
    place_all[0, :, 0:seqs] = jnp.where(routed_t > 0.5, earlier_t, -5000.0)
    for k in range(1, ep):
        remote(place_all.at[0], place_all.at[k], (flip(me, k), t), "place", "place")

    loaded("gains", "proj")
    absorb(res_all.at[0 : tp - 1], arrival("g0"))
    total = jnp.zeros((seqs, 1), f32)
    for j in range(tp):
        part = res_all[j].astype(f32)
        total = total + jnp.sum(part * part, axis=1, keepdims=True)
    scale = lax.rsqrt(total / width + EPSILON)
    mix = jnp.zeros((seqs, chans), f32)
    for j in range(tp):
        xnorm = (res_all[j].astype(f32) * scale * gains[0, j]).astype(bf16)
        mix = mix + dot(xnorm, proj[j * cols : (j + 1) * cols, :])
    mix_f = mix.astype(bf16).astype(f32)
    lane_c = lax.broadcasted_iota(jnp.int32, (seqs, groups, chans), 2)
    group_c = lax.broadcasted_iota(jnp.int32, (seqs, groups, chans), 1)
    first = group_c * group_width
    own = (lane_c >= first) & (lane_c < first + group_width)
    spread = jnp.where(own, jnp.broadcast_to(mix_f[:, None, :], own.shape), 0.0)
    spread = spread.astype(bf16).reshape(seqs * groups, chans)
    drive_re = dot(spread, bb_re).reshape(seqs, groups, states)
    drive_im = dot(spread, bb_im).reshape(seqs, groups, states)
    loaded("state", "read", "skip")
    old_re, old_im = state[0], state[1]
    new_re = abar_re * old_re - abar_im * old_im + drive_re
    new_im = abar_re * old_im + abar_im * old_re + drive_im
    sre_out[...] = new_re
    sim_out[...] = new_im
    flat = (seqs * groups, states)
    readout = lax.dot_general(
        new_re.reshape(flat).astype(bf16), read_maps[0].astype(bf16), last, preferred_element_type=f32
    ) - lax.dot_general(
        new_im.reshape(flat).astype(bf16), read_maps[1].astype(bf16), last, preferred_element_type=f32
    )
    readout = jnp.sum(jnp.where(own, readout.reshape(seqs, groups, chans), 0.0), axis=1)
    pre = readout + skip_ref[...] * mix_f
    mixer = 0.5 * pre * (1.0 + erf(pre * 0.7071067811865476))
    mix_all[t] = mixer.astype(bf16)
    gather(mix_all.at[t], mix_all.at[t], "g1")

    absorb(place_all.at[0 : ep - 1], arrival("place"))
    iota_r = lax.broadcasted_iota(jnp.int32, (rows, seqs), 0).astype(f32)
    iota_l = lax.broadcasted_iota(jnp.int32, (seqs, rows), 1).astype(f32)

    def slot_row(n, b):
        return place_all[2 * n + b, pl.ds(me, 1), 0:seqs] + float((n % 2 * 2 + b) * cap)

    for n in range(chips):
        for b in range(2):
            slots = slot_row(n, b)
            span = slice((n % 2 * 2 + b) * seqs, (n % 2 * 2 + b + 1) * seqs)
            pick[n // 2, :, span] = jnp.where(iota_r == slots, 1.0, 0.0).astype(bf16)
            down = jnp.sum(jnp.where(row_i == col_i, slots, 0.0), axis=1, keepdims=True)
            spill[n, b * seqs : (b + 1) * seqs, :] = jnp.where(iota_l == down, 1.0, 0.0).astype(bf16)

    loaded("glu")
    absorb(mix_all.at[0 : tp - 1], arrival("g1"))
    glu_gate = jnp.zeros((seqs, chans), f32)
    for j in range(tp):
        glu_gate = glu_gate + dot(mix_all[j], glu[j * chans : (j + 1) * chans, :])
    gated_all[t] = (mixer * jax.nn.sigmoid(glu_gate)).astype(bf16)
    gather(gated_all.at[t], gated_all.at[t], "g2")
    loaded("outp", "router")
    absorb(gated_all.at[0 : tp - 1], arrival("g2"))
    mixed = resid_ref[...].astype(f32)
    for j in range(tp):
        mixed = mixed + dot(gated_all[j], outp[j * chans : (j + 1) * chans, :])
    stream = mixed.astype(bf16)
    stream_f = stream.astype(f32)

    tok[0, t, 0:seqs, :] = stream
    top, bottom = pl.ds(0, half), pl.ds(half, half)

    def slab(n, j, b=0, cut=None):
        begin, size = (n % 2) * pair + b * seqs, seqs
        if cut is not None:
            begin, size = begin + cut * half, half
        return tok.at[n // 2, j, pl.ds(begin, size)]

    def to_twin(n, key, j):
        remote(slab(n, j, 0), slab(n, j, 1), twin, "twin", ("twin", n // 2, key))

    def spread_chips():
        for n in range(1, chips):
            remote(slab(0, t), slab(n, t), (flip(me, 2 * n), t), "chips", ("chips", n))

    def enter(n):
        if n:
            absorb(home_in.at[0], arrival(("chips", n)))
        block = slab(n, t)
        if n in direct_in:
            remote(block, block, side_o, "relay", ("corner", n))
        remote(block, block, side_b, "side", ("side", n))
        remote(block, block, side_a, "side", ("side", n))
        to_twin(n, "t", t)

    def relay(n):
        absorb(home_in.at[0:2], arrival(("side", n)))
        if n not in direct_in:
            first_b, second_a = slab(n, beside, 0, 0), slab(n, across, 0, 1)
            remote(first_b, first_b, side_a, "relay", ("corner", n))
            remote(second_a, second_a, side_b, "relay", ("corner", n))
        to_twin(n, "ba", beside)
        to_twin(n, "ba", across)

    def corner(n):
        absorb(home_in.at[0], arrival(("corner", n)))
        to_twin(n, "o", opposite)

    def logits():
        logit_all[t] = jnp.zeros(logit_all.shape[1:], f32)
        logit_all[t, 0:ep, 0:seqs] = lax.dot_general(
            router_ref[:, pl.ds(pl.multiple_of(t * cols, cols), cols)],
            stream_f * gains[1, t],
            last,
            precision=lax.Precision.HIGHEST,
            preferred_element_type=f32,
        )
        energy = jnp.sum(stream_f * stream_f, axis=1, keepdims=True)
        logit_all[t, ep : ep + 1, 0:seqs] = jnp.sum(
            jnp.where(row_i == col_i, energy, 0.0), axis=0, keepdims=True
        )
        gather(logit_all.at[t], logit_all.at[t], "g3")

    def weights():
        absorb(logit_all.at[0 : tp - 1], arrival("g3"))
        whole = logit_all[0]
        for j in range(1, tp):
            whole = whole + logit_all[j]
        whole = whole[:, 0:seqs]
        inverse = lax.rsqrt(whole[ep : ep + 1] / width + EPSILON)
        chosen = routed_t > 0.5
        expon = jnp.where(chosen, jnp.exp(jnp.where(chosen, whole[0:ep] * inverse, 0.0)), 0.0)
        weight_all[0] = jnp.zeros(weight_all.shape[1:], f32)
        weight_all[0, 0:ep, 0:seqs] = expon / jnp.sum(expon, axis=0, keepdims=True)
        weight_all[0, ep : ep + 1, 0:seqs] = inverse
        for k in range(1, ep):
            remote(weight_all.at[0], weight_all.at[k], (flip(me, k), t), "weight", "weight")

    def expert_in(h, key):
        places = {"t": [t], "ba": [beside, across], "o": [opposite]}[key]
        if (h, key) == (0, "t"):
            loaded("gate", "up")
        absorb(res_all.at[0 : 2 * len(places)], arrival(("twin", h, key)))
        total_g = total_u = None
        for j in places:
            scaled = (dot(pick[h], tok[h, j]) * gains[1, j]).astype(bf16)
            span = pl.ds(pl.multiple_of(j * cols, cols), cols)
            part_g, part_u = dot(scaled, wg[span, :]), dot(scaled, wu[span, :])
            total_g = part_g if total_g is None else total_g + part_g
            total_u = part_u if total_u is None else total_u + part_u
        if key == "t":
            acc_g[...] = total_g
            acc_u[...] = total_u
        else:
            acc_g[...] += total_g
            acc_u[...] += total_u

    def activate(h):
        if h == 0:
            absorb(weight_all.at[0 : ep - 1], arrival("weight"))
        norm = jnp.zeros((rows, 1), f32)
        share = jnp.zeros((rows, 1), f32)
        for n in (2 * h, 2 * h + 1):
            for b in range(2):
                match = iota_r == slot_row(n, b)
                inverse = weight_all[2 * n + b, ep : ep + 1, 0:seqs]
                weight = weight_all[2 * n + b, pl.ds(me, 1), 0:seqs]
                norm = norm + jnp.sum(jnp.where(match, inverse, 0.0), axis=1, keepdims=True)
                share = share + jnp.sum(jnp.where(match, weight, 0.0), axis=1, keepdims=True)
        gate_cl = jnp.minimum(acc_g[...] * norm, LIMIT)
        up_cl = jnp.clip(acc_u[...] * norm, -LIMIT, LIMIT)
        act[h] = (((up_cl + 1.0) * share) * (gate_cl * jax.nn.sigmoid(ALPHA * gate_cl))).astype(bf16)

    def expert_out(n):
        if n == outs[0]:
            loaded("down")
        spread_act = dot(spill[n], act[n // 2]).astype(bf16)
        order = (opposite, beside, across, t)
        for j in order:
            value = dot(spread_act, wd[j])
            sib_out[n, j] = value[seqs:].astype(bf16)
            mine[n, j] = value[:seqs]
        remote(sib_out.at[n], sib_in.at[n], twin, "back", ("back", n))

    def reduce_chip(n):
        absorb(sib_in.at[n], arrival(("back", n)))
        for j in (opposite, beside, across):
            both = mine[n, j] + sib_in[n, j].astype(f32)
            mine[n, j] = both
            summed[n, j] = both.astype(bf16)
        if n in direct_out:
            remote(summed.at[n, opposite], from_side.at[n, 2], side_o, "sum", ("mine", n))
            remote(summed.at[n, beside], from_side.at[n, 0], side_b, "sum", ("mine", n))
            remote(summed.at[n, across], from_side.at[n, 1], side_a, "sum", ("mine", n))
            return
        remote(summed.at[n, opposite, top], fwd_in.at[n, 0], side_b, "sum", ("fwd", n))
        remote(summed.at[n, opposite, bottom], fwd_in.at[n, 1], side_a, "sum", ("fwd", n))
        remote(summed.at[n, beside, top], from_side.at[n, 0, top], side_b, "sum", ("mine", n))
        remote(summed.at[n, across, bottom], from_side.at[n, 1, bottom], side_a, "sum", ("mine", n))

    def reduce_relay(n):
        if n in direct_out:
            return
        absorb(fwd_in.at[n], arrival(("fwd", n)))
        fwd_out[n, 0] = (mine[n, across, 0:half] + fwd_in[n, 0].astype(f32)).astype(bf16)
        fwd_out[n, 1] = (mine[n, beside, half:] + fwd_in[n, 1].astype(f32)).astype(bf16)
        remote(fwd_out.at[n, 0], from_side.at[n, 1, top], side_a, "sum", ("mine", n))
        remote(fwd_out.at[n, 1], from_side.at[n, 0, bottom], side_b, "sum", ("mine", n))

    def go_home(n):
        value = mine[n, t] + sib_in[n, t].astype(f32)
        count = 3 if n in direct_out else 2
        absorb(from_side.at[n, 0:count], arrival(("mine", n)))
        for k in range(count):
            value = value + from_side[n, k].astype(f32)
        if n:
            home_out[n] = value.astype(bf16)
            remote(home_out.at[n], home_in.at[n], (flip(me, 2 * n), t), "home", "home")
        else:
            mine[n, t] = value

    def finish():
        result = stream_f + mine[0, t]
        absorb(home_in.at[0 : chips - 1], arrival("home"))
        for n in range(1, chips):
            result = result + home_in[n].astype(f32)
        out_ref[...] = result.astype(bf16)

    direct_in, direct_out = (), ()
    outs = (1, 0, 3, 2)
    plan = [
        (spread_chips,), (enter, 0), (logits,),
        (relay, 0), (enter, 1), (weights,), (enter, 2), (corner, 0), (relay, 1),
        (expert_in, 0, "t"), (enter, 3), (relay, 2), (corner, 1), (expert_in, 0, "ba"),
        (expert_in, 0, "o"), (relay, 3), (corner, 2), (activate, 0), (expert_out, 1), (expert_out, 0), (corner, 3),
        (expert_in, 1, "t"), (reduce_chip, 1), (expert_in, 1, "ba"), (reduce_chip, 0), (expert_in, 1, "o"), (activate, 1),
        (reduce_relay, 1), (expert_out, 3), (reduce_relay, 0), (expert_out, 2), (go_home, 1), (reduce_chip, 3), (go_home, 0), (reduce_chip, 2),
        (reduce_relay, 3), (reduce_relay, 2), (go_home, 3), (go_home, 2),
        (finish,),
    ]
    for step in plan:
        step[0](*step[1:])
    spent = {
        "g0": res_all.at[0 : tp - 1],
        "g1": mix_all.at[0 : tp - 1],
        "g2": gated_all.at[0 : tp - 1],
        "g3": logit_all.at[0 : tp - 1],
        "place": place_all.at[0 : ep - 1],
        "weight": weight_all.at[0 : ep - 1],
        "chips": home_in.at[0 : chips - 1],
        "side": tok.at[0, 0 : chips // 2],
        "relay": tok.at[0, 0],
        "twin": tok.at[0, 0:chips],
        "back": sib_in,
        "home": home_in.at[0 : chips - 1],
    }
    for kind, ref in spent.items():
        absorb(ref, send_sem.at[SENDS.index(kind)])
    absorb(sib_in.at[:, 0:3], send_sem.at[SENDS.index("sum")])


def finish_kernel(a_in, b_in, c_in, a_out, b_out, c_out, sems):
    writes = [
        pltpu.make_async_copy(held, target, sems.at[n])
        for n, (held, target) in enumerate(((a_in, a_out), (b_in, b_out), (c_in, c_out)))
    ]
    for write in writes:
        write.start()
    for write in writes:
        write.wait()


def dispatch(*args):
    (
        residual, state_re, state_im, mix_gain, proj_in, decay_rate, frequency, log_step,
        input_re, input_im, read_re, read_im, skip_gain, glu_weight, out_proj, ffn_gain,
        router, gate_weight, up_weight, down_weight, route_ids,
    ) = args
    ep, tp = lax.axis_size("ep"), lax.axis_size("tp")
    seqs, cols = residual.shape
    groups, states = decay_rate.shape
    chans = skip_gain.shape[0]
    rough = groups % 16 or chans % 128 or cols % 128 or seqs % 32 or seqs > 128
    if gate_weight.shape[0] != 1 or tp != 4 or ep != 8 or rough:
        return per_device(*args)
    top = route_ids.shape[1]
    cap = seqs * top // router.shape[1] + 1
    rows = -(-4 * cap // 16) * 16
    hidden = gate_weight.shape[2]
    width = mix_gain.shape[0]
    chips = ep // 2
    halves = chips // 2
    bf16, f32 = jnp.bfloat16, jnp.float32
    hbm, vmem = pl.BlockSpec(memory_space=pltpu.HBM), pl.BlockSpec(memory_space=pltpu.VMEM)
    state_shape = (seqs, groups, states)
    blocks = (chips, tp, seqs, cols)
    out = pl.pallas_call(
        functools.partial(layer_kernel, (ep, tp, cap, rows)),
        out_shape=(
            pltpu.VMEM((seqs, cols), bf16),
            pltpu.VMEM(state_shape, f32),
            pltpu.VMEM(state_shape, f32),
        ),
        in_specs=[hbm] * 21,
        out_specs=(vmem, vmem, vmem),
        scratch_shapes=[
            pltpu.VMEM((seqs, cols), bf16),
            pltpu.VMEM((2, tp, 1, cols), f32),
            pltpu.VMEM((2, groups, states), f32),
            pltpu.VMEM((1, groups), f32),
            pltpu.VMEM((2, groups, chans // groups, states), f32),
            pltpu.VMEM((2, chans, states), f32),
            pltpu.VMEM((1, chans), f32),
            pltpu.VMEM((ep, width), f32),
            pltpu.VMEM((top, seqs), jnp.int32),
            pltpu.VMEM((2,) + state_shape, f32),
            pltpu.VMEM(proj_in.shape, bf16),
            pltpu.VMEM(glu_weight.shape, bf16),
            pltpu.VMEM(out_proj.shape, bf16),
            pltpu.VMEM(gate_weight.shape[1:], bf16),
            pltpu.VMEM(up_weight.shape[1:], bf16),
            pltpu.VMEM((tp, hidden, cols), bf16),
            pltpu.VMEM((tp, seqs, cols), bf16),
            pltpu.VMEM((tp, seqs, chans), bf16),
            pltpu.VMEM((tp, seqs, chans), bf16),
            pltpu.VMEM((tp, 2 * ep, 128), f32),
            pltpu.VMEM((ep, ep, 128), f32),
            pltpu.VMEM((ep, 2 * ep, 128), f32),
            pltpu.VMEM((halves, rows, 4 * seqs), bf16),
            pltpu.VMEM((chips, 2 * seqs, rows), bf16),
            pltpu.VMEM((halves, tp, 4 * seqs, cols), bf16),
            pltpu.VMEM((rows, hidden), f32),
            pltpu.VMEM((rows, hidden), f32),
            pltpu.VMEM((halves, rows, hidden), bf16),
            pltpu.VMEM(blocks, f32),
            pltpu.VMEM(blocks, bf16),
            pltpu.VMEM(blocks, bf16),
            pltpu.VMEM(blocks, bf16),
            pltpu.VMEM((chips, 3, seqs, cols), bf16),
            pltpu.VMEM((chips, 2, seqs // 2, cols), bf16),
            pltpu.VMEM((chips, 2, seqs // 2, cols), bf16),
            pltpu.VMEM((chips, seqs, cols), bf16),
            pltpu.VMEM((chips, seqs, cols), bf16),
            pltpu.SemaphoreType.DMA((16,)),
            pltpu.SemaphoreType.DMA((len(SENDS),)),
            pltpu.SemaphoreType.DMA((44,)),
        ],
        compiler_params=pltpu.CompilerParams(
            collective_id=0, has_side_effects=True, vmem_limit_bytes=48 * 1024 * 1024
        ),
        name="layer",
    )(*(pltpu.with_memory_space_constraint(part, pltpu.HBM) for part in (
        residual,
        mix_gain.reshape(tp, 1, cols),
        ffn_gain.reshape(tp, 1, cols),
        decay_rate,
        frequency,
        log_step.reshape(1, groups),
        input_re.transpose(0, 2, 1),
        input_im.transpose(0, 2, 1),
        read_re.reshape(chans, states),
        read_im.reshape(chans, states),
        skip_gain.reshape(1, chans),
        router.T,
        route_ids.T,
        state_re,
        state_im,
        proj_in,
        glu_weight,
        out_proj,
        gate_weight.reshape(gate_weight.shape[1:]),
        up_weight.reshape(up_weight.shape[1:]),
        down_weight.reshape(down_weight.shape[1:]),
    )))
    return pl.pallas_call(
        finish_kernel,
        out_shape=tuple(jax.ShapeDtypeStruct(part.shape, part.dtype) for part in out),
        in_specs=[vmem] * 3,
        out_specs=(hbm,) * 3,
        scratch_shapes=[pltpu.SemaphoreType.DMA((3,))],
        compiler_params=pltpu.CompilerParams(vmem_limit_bytes=8 * 1024 * 1024),
        name="finish",
    )(*out)


def solution(mesh):
    in_specs = (
        P("ep", "tp"),
        P("ep", "tp", None),
        P("ep", "tp", None),
        P(),
        P(None, "tp"),
        P("tp", None),
        P("tp", None),
        P("tp"),
        P("tp", None, None),
        P("tp", None, None),
        P("tp", None, None),
        P("tp", None, None),
        P("tp"),
        P(None, "tp"),
        P(None, "tp"),
        P(),
        P(),
        P("ep", None, "tp"),
        P("ep", None, "tp"),
        P("ep", "tp", None),
        P("ep", None),
    )
    out_specs = (P("ep", "tp"), P("ep", "tp", None), P("ep", "tp", None))
    return jax.shard_map(
        dispatch, mesh=mesh, in_specs=in_specs, out_specs=out_specs, check_vma=False
    )
```

time: 66.4 us -> 56.2 us (0.85)
  Pallas kernels: 65.6 us -> 55.4 us
    pallas_call x1, Pallas kernels: 63.5 us -> 54.4 us  [dispatch(): pl.pallas_call(functools.partial(layer_kernel, (ep, tp, cap, rows)), out_...]
    pallas_call x1, Pallas kernels: 2.1 us -> 1.02 us  [dispatch(): pl.pallas_call(finish_kernel, out_shape=tuple((jax.ShapeDtypeStruct(part....]
where the time goes in v2:
time: 56.2 us; the launch traced here: 56.1 us
  Pallas kernels  55.4 us (99%)
  between operations  0.65 us (1%)
    pallas_call x1, Pallas kernels, dispatch(): pl.pallas_call(functools.partial(layer_kernel, (ep, tp, cap, rows)), out_...  54.4 us

profile of v2, /device:TPU:0, one launch (start us, length us, event | category | flops | bytes accessed | tf_op | source)
XLA Modules:
  0.0 56.1 jit_solution(11882351185775228165)
XLA Ops:
  0.6 54.4 %layer.1 = (bf16[64,512]{1,0:T(8,128)(2,1)S(1)}, f32[64,16,64]{2,1,0:T(8,128)S(1)}, f32[64,16,64]{2,1,0:T(8,128)S(1)}) custom-call(bf16[64,512]{1,0:T(8,128)(2,1)} %resid_hbm.1, f32[4,1,512]{2,1,0:T(1,128)} %bitcast.21, f32[4,1,512]{2,1,0:T(1,128)} %bitcast.22, f32[16,64]{1,0:T(8,128)} %decay_hbm.1, f32[16,64]{1,0:T(8,128)} %freq_hbm.1, f32[1,16]{1,0:T(1,128)} %bitcast.25, ...), custom_call_target="tpu_custom_call" | custom-call | tf_op jit(solution)/shard_map/layer/pallas_call | solution.py:653
  55.0 1.0 %finish.1 = (bf16[64,512]{1,0:T(8,128)(2,1)}, f32[64,16,64]{2,1,0:T(8,128)}, f32[64,16,64]{2,1,0:T(8,128)}) custom-call(bf16[64,512]{1,0:T(8,128)(2,1)S(1)} %get-tuple-element.6.a_in, f32[64,16,64]{2,1,0:T(8,128)S(1)} %get-tuple-element.7.b_in, f32[64,16,64]{2,1,0:T(8,128)S(1)} %get-tuple-element.8.c_in), custom_call_target="tpu_custom_call" | custom-call | tf_op jit(solution)/shard_map/finish/pallas_call | solution.py:731

commit v3 on v2

--- a/solution.py
+++ b/solution.py
@@ -162,7 +162,7 @@
     return x * top / bottom
 
 
-SENDS = ("g0", "g1", "g2", "g3", "place", "weight", "chips", "side", "relay", "twin", "back", "sum", "home")
+SENDS = ("g0", "g1", "g2", "g3", "weight", "chips", "side", "relay", "twin", "back", "sum", "home")
 
 
 def layer_kernel(
@@ -204,20 +204,16 @@
     proj,
     glu,
     outp,
-    wg,
-    wu,
+    wgu,
     wd,
     res_all,
     mix_all,
     gated_all,
     logit_all,
-    place_all,
     weight_all,
-    pick,
-    spill,
     tok,
-    acc_g,
-    acc_u,
+    ready,
+    acc,
     act,
     mine,
     sib_out,
@@ -232,7 +228,8 @@
     send_sem,
     recv_sem,
 ):
-    ep, tp, cap, rows = sizes
+    ep, tp = sizes
+    rows = 2 * resid_ref.shape[0]
     f32, bf16 = jnp.float32, jnp.bfloat16
     me, t = lax.axis_index("ep"), lax.axis_index("tp")
     seqs, cols = resid_ref.shape
@@ -241,8 +238,8 @@
     chans = skip_ref.shape[1]
     group_width = chans // groups
     chips = ep // 2
-    pair = 2 * seqs
     half = seqs // 2
+    hidden = wd.shape[1]
     last = (((1,), (1,)), ((), ()))
 
     def dot(a, b):
@@ -262,8 +259,7 @@
         "glu": (glu, [(glu_hbm, glu)]),
         "outp": (outp, [(outp_hbm, outp)]),
         "router": (router_ref, [(router_hbm, router_ref)]),
-        "gate": (wg, [(gate_hbm, wg)]),
-        "up": (wu, [(up_hbm, wu)]),
+        "experts": (wgu, [(gate_hbm, wgu.at[:, 0:hidden]), (up_hbm, wgu.at[:, hidden : 2 * hidden])]),
         "down": (wd, [(down_hbm.at[:, j * cols : (j + 1) * cols], wd.at[j]) for j in range(tp)]),
     }
     names = list(batches)
@@ -349,11 +345,6 @@
         routed_t = routed_t + jnp.where(route[j : j + 1, :] == iota_e, 1.0, 0.0)
     row_i = lax.broadcasted_iota(jnp.int32, (seqs, seqs), 0)
     col_i = lax.broadcasted_iota(jnp.int32, (seqs, seqs), 1)
-    earlier_t = dot(routed_t.astype(bf16), jnp.where(row_i < col_i, 1.0, 0.0).astype(bf16))
-    place_all[0] = jnp.zeros(place_all.shape[1:], f32)
-    place_all[0, :, 0:seqs] = jnp.where(routed_t > 0.5, earlier_t, -5000.0)
-    for k in range(1, ep):
-        remote(place_all.at[0], place_all.at[k], (flip(me, k), t), "place", "place")
 
     loaded("gains", "proj")
     absorb(res_all.at[0 : tp - 1], arrival("g0"))
@@ -393,21 +384,6 @@
     mix_all[t] = mixer.astype(bf16)
     gather(mix_all.at[t], mix_all.at[t], "g1")
 
-    absorb(place_all.at[0 : ep - 1], arrival("place"))
-    iota_r = lax.broadcasted_iota(jnp.int32, (rows, seqs), 0).astype(f32)
-    iota_l = lax.broadcasted_iota(jnp.int32, (seqs, rows), 1).astype(f32)
-
-    def slot_row(n, b):
-        return place_all[2 * n + b, pl.ds(me, 1), 0:seqs] + float((n % 2 * 2 + b) * cap)
-
-    for n in range(chips):
-        for b in range(2):
-            slots = slot_row(n, b)
-            span = slice((n % 2 * 2 + b) * seqs, (n % 2 * 2 + b + 1) * seqs)
-            pick[n // 2, :, span] = jnp.where(iota_r == slots, 1.0, 0.0).astype(bf16)
-            down = jnp.sum(jnp.where(row_i == col_i, slots, 0.0), axis=1, keepdims=True)
-            spill[n, b * seqs : (b + 1) * seqs, :] = jnp.where(iota_l == down, 1.0, 0.0).astype(bf16)
-
     loaded("glu")
     absorb(mix_all.at[0 : tp - 1], arrival("g1"))
     glu_gate = jnp.zeros((seqs, chans), f32)
@@ -427,13 +403,13 @@
     top, bottom = pl.ds(0, half), pl.ds(half, half)
 
     def slab(n, j, b=0, cut=None):
-        begin, size = (n % 2) * pair + b * seqs, seqs
+        begin, size = b * seqs, seqs
         if cut is not None:
             begin, size = begin + cut * half, half
-        return tok.at[n // 2, j, pl.ds(begin, size)]
+        return tok.at[n, j, pl.ds(begin, size)]
 
     def to_twin(n, key, j):
-        remote(slab(n, j, 0), slab(n, j, 1), twin, "twin", ("twin", n // 2, key))
+        remote(slab(n, j, 0), slab(n, j, 1), twin, "twin", ("twin", n, key))
 
     def spread_chips():
         for n in range(1, chips):
@@ -492,58 +468,76 @@
         for k in range(1, ep):
             remote(weight_all.at[0], weight_all.at[k], (flip(me, k), t), "weight", "weight")
 
-    def expert_in(h, key):
-        places = {"t": [t], "ba": [beside, across], "o": [opposite]}[key]
-        if (h, key) == (0, "t"):
-            loaded("gate", "up")
-        absorb(res_all.at[0 : 2 * len(places)], arrival(("twin", h, key)))
-        total_g = total_u = None
-        for j in places:
-            scaled = (dot(pick[h], tok[h, j]) * gains[1, j]).astype(bf16)
-            span = pl.ds(pl.multiple_of(j * cols, cols), cols)
-            part_g, part_u = dot(scaled, wg[span, :]), dot(scaled, wu[span, :])
-            total_g = part_g if total_g is None else total_g + part_g
-            total_u = part_u if total_u is None else total_u + part_u
-        if key == "t":
-            acc_g[...] = total_g
-            acc_u[...] = total_u
-        else:
-            acc_g[...] += total_g
-            acc_u[...] += total_u
-
-    def activate(h):
-        if h == 0:
+    def scale_in(n, key):
+        for name, places in (("t", [t]), ("ba", [beside, across]), ("o", [opposite])):
+            if name not in key:
+                continue
+            absorb(res_all.at[0 : len(places)], arrival(("twin", n, name)))
+            for j in places:
+                span = pl.ds(pl.multiple_of(j * cols, cols), cols)
+                ready[n, :, span] = (tok[n, j].astype(f32) * gains[1, j]).astype(bf16)
+
+    def expert_in(n):
+        if n == outs[0]:
+            loaded("experts")
+        acc[...] = dot(ready[n], wgu[...])
+
+    def column(line):
+        return jnp.sum(jnp.where(row_i == col_i, line, 0.0), axis=1, keepdims=True)
+
+    def activate(n):
+        if n == outs[0]:
             absorb(weight_all.at[0 : ep - 1], arrival("weight"))
-        norm = jnp.zeros((rows, 1), f32)
-        share = jnp.zeros((rows, 1), f32)
-        for n in (2 * h, 2 * h + 1):
-            for b in range(2):
-                match = iota_r == slot_row(n, b)
-                inverse = weight_all[2 * n + b, ep : ep + 1, 0:seqs]
-                weight = weight_all[2 * n + b, pl.ds(me, 1), 0:seqs]
-                norm = norm + jnp.sum(jnp.where(match, inverse, 0.0), axis=1, keepdims=True)
-                share = share + jnp.sum(jnp.where(match, weight, 0.0), axis=1, keepdims=True)
-        gate_cl = jnp.minimum(acc_g[...] * norm, LIMIT)
-        up_cl = jnp.clip(acc_u[...] * norm, -LIMIT, LIMIT)
-        act[h] = (((up_cl + 1.0) * share) * (gate_cl * jax.nn.sigmoid(ALPHA * gate_cl))).astype(bf16)
+        for b in range(2):
+            lines = slice(b * seqs, (b + 1) * seqs)
+            norm = column(weight_all[2 * n + b, ep : ep + 1, 0:seqs])
+            share = column(weight_all[2 * n + b, pl.ds(me, 1), 0:seqs])
+            gate_cl = jnp.minimum(acc[lines, 0:hidden] * norm, LIMIT)
+            up_cl = jnp.clip(acc[lines, hidden:] * norm, -LIMIT, LIMIT)
+            act[n, lines] = (((up_cl + 1.0) * share) * (gate_cl * jax.nn.sigmoid(ALPHA * gate_cl))).astype(bf16)
 
     def expert_out(n):
         if n == outs[0]:
             loaded("down")
-        spread_act = dot(spill[n], act[n // 2]).astype(bf16)
-        order = (opposite, beside, across, t)
-        for j in order:
-            value = dot(spread_act, wd[j])
+        for number, j in enumerate((opposite, beside, across, t)):
+            value = dot(act[n], wd[j])
             sib_out[n, j] = value[seqs:].astype(bf16)
             mine[n, j] = value[:seqs]
-        remote(sib_out.at[n], sib_in.at[n], twin, "back", ("back", n))
+            if number == 0 and n in early_out:
+                remote(sib_out.at[n, j], sib_in.at[n, j], twin, "back", ("corner back", n))
+        if n in early_out:
+            for j in (beside, across, t):
+                remote(sib_out.at[n, j], sib_in.at[n, j], twin, "back", ("back", n))
+        else:
+            remote(sib_out.at[n], sib_in.at[n], twin, "back", ("back", n))
+
+    def add_twin(n, j):
+        both = mine[n, j] + sib_in[n, j].astype(f32)
+        mine[n, j] = both
+        summed[n, j] = both.astype(bf16)
 
     def reduce_chip(n):
+        if n in early_out:
+            absorb(sib_in.at[n, 0], arrival(("corner back", n)))
+            add_twin(n, opposite)
+            if n not in direct_out:
+                remote(summed.at[n, opposite, top], fwd_in.at[n, 0], side_b, "sum", ("fwd", n))
+                remote(summed.at[n, opposite, bottom], fwd_in.at[n, 1], side_a, "sum", ("fwd", n))
+            else:
+                remote(summed.at[n, opposite], from_side.at[n, 2], side_o, "sum", ("mine", n))
+            absorb(sib_in.at[n, 0 : tp - 1], arrival(("back", n)))
+            add_twin(n, beside)
+            add_twin(n, across)
+            if n in direct_out:
+                remote(summed.at[n, beside], from_side.at[n, 0], side_b, "sum", ("mine", n))
+                remote(summed.at[n, across], from_side.at[n, 1], side_a, "sum", ("mine", n))
+            else:
+                remote(summed.at[n, beside, top], from_side.at[n, 0, top], side_b, "sum", ("mine", n))
+                remote(summed.at[n, across, bottom], from_side.at[n, 1, bottom], side_a, "sum", ("mine", n))
+            return
         absorb(sib_in.at[n], arrival(("back", n)))
         for j in (opposite, beside, across):
-            both = mine[n, j] + sib_in[n, j].astype(f32)
-            mine[n, j] = both
-            summed[n, j] = both.astype(bf16)
+            add_twin(n, j)
         if n in direct_out:
             remote(summed.at[n, opposite], from_side.at[n, 2], side_o, "sum", ("mine", n))
             remote(summed.at[n, beside], from_side.at[n, 0], side_b, "sum", ("mine", n))
@@ -583,15 +577,15 @@
         out_ref[...] = result.astype(bf16)
 
     direct_in, direct_out = (), ()
-    outs = (1, 0, 3, 2)
+    outs, early_out = (0, 1, 2, 3), (3,)
     plan = [
         (spread_chips,), (enter, 0), (logits,),
-        (relay, 0), (enter, 1), (weights,), (enter, 2), (corner, 0), (relay, 1),
-        (expert_in, 0, "t"), (enter, 3), (relay, 2), (corner, 1), (expert_in, 0, "ba"),
-        (expert_in, 0, "o"), (relay, 3), (corner, 2), (activate, 0), (expert_out, 1), (expert_out, 0), (corner, 3),
-        (expert_in, 1, "t"), (reduce_chip, 1), (expert_in, 1, "ba"), (reduce_chip, 0), (expert_in, 1, "o"), (activate, 1),
-        (reduce_relay, 1), (expert_out, 3), (reduce_relay, 0), (expert_out, 2), (go_home, 1), (reduce_chip, 3), (go_home, 0), (reduce_chip, 2),
-        (reduce_relay, 3), (reduce_relay, 2), (go_home, 3), (go_home, 2),
+        (relay, 0), (enter, 1), (enter, 2), (weights,), (scale_in, 0, "t"), (corner, 0), (scale_in, 0, "ba"), (scale_in, 1, "t"), (relay, 1), (enter, 3),
+        (scale_in, 0, "o"), (expert_in, 0), (relay, 2), (activate, 0), (scale_in, 1, "ba"), (corner, 1), (expert_out, 0), (relay, 3), (scale_in, 2, "t"), (scale_in, 2, "ba"), (scale_in, 1, "o"),
+        (expert_in, 1), (corner, 2), (reduce_chip, 0), (activate, 1), (expert_out, 1), (scale_in, 3, "t"), (corner, 3), (scale_in, 3, "ba"),
+        (scale_in, 2, "o"), (expert_in, 2), (reduce_chip, 1), (activate, 2), (expert_out, 2), (reduce_relay, 0),
+        (scale_in, 3, "o"), (expert_in, 3), (reduce_chip, 2), (activate, 3), (expert_out, 3), (reduce_relay, 1), (go_home, 0),
+        (reduce_chip, 3), (reduce_relay, 2), (go_home, 1), (reduce_relay, 3), (go_home, 2), (go_home, 3),
         (finish,),
     ]
     for step in plan:
@@ -601,12 +595,11 @@
         "g1": mix_all.at[0 : tp - 1],
         "g2": gated_all.at[0 : tp - 1],
         "g3": logit_all.at[0 : tp - 1],
-        "place": place_all.at[0 : ep - 1],
         "weight": weight_all.at[0 : ep - 1],
         "chips": home_in.at[0 : chips - 1],
-        "side": tok.at[0, 0 : chips // 2],
-        "relay": tok.at[0, 0],
-        "twin": tok.at[0, 0:chips],
+        "side": tok.at[0],
+        "relay": tok.at[0, 0 : tp // 2],
+        "twin": tok.at[0:2],
         "back": sib_in,
         "home": home_in.at[0 : chips - 1],
     }
@@ -640,18 +633,15 @@
     if gate_weight.shape[0] != 1 or tp != 4 or ep != 8 or rough:
         return per_device(*args)
     top = route_ids.shape[1]
-    cap = seqs * top // router.shape[1] + 1
-    rows = -(-4 * cap // 16) * 16
     hidden = gate_weight.shape[2]
     width = mix_gain.shape[0]
     chips = ep // 2
-    halves = chips // 2
     bf16, f32 = jnp.bfloat16, jnp.float32
     hbm, vmem = pl.BlockSpec(memory_space=pltpu.HBM), pl.BlockSpec(memory_space=pltpu.VMEM)
     state_shape = (seqs, groups, states)
     blocks = (chips, tp, seqs, cols)
     out = pl.pallas_call(
-        functools.partial(layer_kernel, (ep, tp, cap, rows)),
+        functools.partial(layer_kernel, (ep, tp)),
         out_shape=(
             pltpu.VMEM((seqs, cols), bf16),
             pltpu.VMEM(state_shape, f32),
@@ -673,21 +663,17 @@
             pltpu.VMEM(proj_in.shape, bf16),
             pltpu.VMEM(glu_weight.shape, bf16),
             pltpu.VMEM(out_proj.shape, bf16),
-            pltpu.VMEM(gate_weight.shape[1:], bf16),
-            pltpu.VMEM(up_weight.shape[1:], bf16),
+            pltpu.VMEM((width, 2 * hidden), bf16),
             pltpu.VMEM((tp, hidden, cols), bf16),
             pltpu.VMEM((tp, seqs, cols), bf16),
             pltpu.VMEM((tp, seqs, chans), bf16),
             pltpu.VMEM((tp, seqs, chans), bf16),
             pltpu.VMEM((tp, 2 * ep, 128), f32),
-            pltpu.VMEM((ep, ep, 128), f32),
             pltpu.VMEM((ep, 2 * ep, 128), f32),
-            pltpu.VMEM((halves, rows, 4 * seqs), bf16),
-            pltpu.VMEM((chips, 2 * seqs, rows), bf16),
-            pltpu.VMEM((halves, tp, 4 * seqs, cols), bf16),
-            pltpu.VMEM((rows, hidden), f32),
-            pltpu.VMEM((rows, hidden), f32),
-            pltpu.VMEM((halves, rows, hidden), bf16),
+            pltpu.VMEM((chips, tp, 2 * seqs, cols), bf16),
+            pltpu.VMEM((chips, 2 * seqs, width), bf16),
+            pltpu.VMEM((2 * seqs, 2 * hidden), f32),
+            pltpu.VMEM((chips, 2 * seqs, hidden), bf16),
             pltpu.VMEM(blocks, f32),
             pltpu.VMEM(blocks, bf16),
             pltpu.VMEM(blocks, bf16),
@@ -697,9 +683,9 @@
             pltpu.VMEM((chips, 2, seqs // 2, cols), bf16),
             pltpu.VMEM((chips, seqs, cols), bf16),
             pltpu.VMEM((chips, seqs, cols), bf16),
-            pltpu.SemaphoreType.DMA((16,)),
+            pltpu.SemaphoreType.DMA((15,)),
             pltpu.SemaphoreType.DMA((len(SENDS),)),
-            pltpu.SemaphoreType.DMA((44,)),
+            pltpu.SemaphoreType.DMA((42,)),
         ],
         compiler_params=pltpu.CompilerParams(
             collective_id=0, has_side_effects=True, vmem_limit_bytes=48 * 1024 * 1024

time: 56.2 us -> 52.5 us (0.934)
  Pallas kernels: 55.4 us -> 51.7 us
    pallas_call x1, Pallas kernels: 54.4 us -> 50.7 us  [dispatch(): pl.pallas_call(functools.partial(layer_kernel, (ep, tp)), out_shape=(pltp...]
where the time goes in v3:
time: 52.5 us; the launch traced here: 52.4 us
  Pallas kernels  51.7 us (98%)
  between operations  0.65 us (1%)
    pallas_call x1, Pallas kernels, dispatch(): pl.pallas_call(functools.partial(layer_kernel, (ep, tp)), out_shape=(pltp...  50.7 us

profile of v3, /device:TPU:0, one launch (start us, length us, event | category | flops | bytes accessed | tf_op | source)
XLA Modules:
  0.0 52.4 jit_solution(1583603068959052754)
XLA Ops:
  0.6 50.7 %layer.1 = (bf16[64,512]{1,0:T(8,128)(2,1)S(1)}, f32[64,16,64]{2,1,0:T(8,128)S(1)}, f32[64,16,64]{2,1,0:T(8,128)S(1)}) custom-call(bf16[64,512]{1,0:T(8,128)(2,1)} %resid_hbm.1, f32[4,1,512]{2,1,0:T(1,128)} %bitcast.21, f32[4,1,512]{2,1,0:T(1,128)} %bitcast.22, f32[16,64]{1,0:T(8,128)} %decay_hbm.1, f32[16,64]{1,0:T(8,128)} %freq_hbm.1, f32[1,16]{1,0:T(1,128)} %bitcast.25, ...), custom_call_target="tpu_custom_call" | custom-call | tf_op jit(solution)/shard_map/layer/pallas_call | solution.py:643
  51.4 1.0 %finish.1 = (bf16[64,512]{1,0:T(8,128)(2,1)}, f32[64,16,64]{2,1,0:T(8,128)}, f32[64,16,64]{2,1,0:T(8,128)}) custom-call(bf16[64,512]{1,0:T(8,128)(2,1)S(1)} %get-tuple-element.6.a_in, f32[64,16,64]{2,1,0:T(8,128)S(1)} %get-tuple-element.7.b_in, f32[64,16,64]{2,1,0:T(8,128)S(1)} %get-tuple-element.8.c_in), custom_call_target="tpu_custom_call" | custom-call | tf_op jit(solution)/shard_map/finish/pallas_call | solution.py:717

commit v4 on v3

--- a/solution.py
+++ b/solution.py
@@ -162,7 +162,7 @@
     return x * top / bottom
 
 
-SENDS = ("g0", "g1", "g2", "g3", "weight", "chips", "side", "relay", "twin", "back", "sum", "home")
+SENDS = ("rows", "g3", "weight")
 
 
 def layer_kernel(
@@ -285,6 +285,16 @@
     arrivals = []
 
     def arrival(key):
+        if key[0] == "fwd":
+            key = ("side", key[1], 0)
+        elif key[0] == "corner back":
+            key = ("side", key[1], 1)
+        elif key[0] == "back":
+            key = ("corner", key[1])
+        elif key[0] == "mine":
+            key = ("g%d" % (key[1] // 2), key[1] % 2)
+        elif key == "home":
+            key = ("g2", 0)
         if key not in arrivals:
             arrivals.append(key)
         return recv_sem.at[arrivals.index(key)]
@@ -293,7 +303,7 @@
         pltpu.make_async_remote_copy(
             src_ref=source,
             dst_ref=target,
-            send_sem=send_sem.at[SENDS.index(kind)],
+            send_sem=send_sem.at[SENDS.index(kind if kind in SENDS else SENDS[0])],
             recv_sem=arrival(key),
             device_id=peer,
             device_id_type=pl.DeviceIdType.MESH,
@@ -310,12 +320,15 @@
     sibling = flip(me, 1)
     side_b, side_a, side_o, twin = (me, beside), (me, across), (me, opposite), (sibling, t)
 
-    def gather(source, target, name):
+    def gather(source, target, kind, key):
         for k in (3, 1, 2):
-            remote(source, target, (me, flip(t, k)), name, name)
+            remote(source, target, (me, flip(t, k)), kind, key)
+
+    halves = [pl.ds(h * half, half) for h in range(2)]
 
     loaded("resid")
-    gather(resid_ref, res_all.at[t], "g0")
+    for h in range(2):
+        gather(resid_ref.at[halves[h]], res_all.at[t, halves[h]], "g0", ("g0", h))
     res_all[t] = resid_ref[...]
 
     loaded("route", "step", "poles", "in")
@@ -346,99 +359,101 @@
     row_i = lax.broadcasted_iota(jnp.int32, (seqs, seqs), 0)
     col_i = lax.broadcasted_iota(jnp.int32, (seqs, seqs), 1)
 
-    loaded("gains", "proj")
-    absorb(res_all.at[0 : tp - 1], arrival("g0"))
-    total = jnp.zeros((seqs, 1), f32)
-    for j in range(tp):
-        part = res_all[j].astype(f32)
-        total = total + jnp.sum(part * part, axis=1, keepdims=True)
-    scale = lax.rsqrt(total / width + EPSILON)
-    mix = jnp.zeros((seqs, chans), f32)
-    for j in range(tp):
-        xnorm = (res_all[j].astype(f32) * scale * gains[0, j]).astype(bf16)
-        mix = mix + dot(xnorm, proj[j * cols : (j + 1) * cols, :])
-    mix_f = mix.astype(bf16).astype(f32)
-    lane_c = lax.broadcasted_iota(jnp.int32, (seqs, groups, chans), 2)
-    group_c = lax.broadcasted_iota(jnp.int32, (seqs, groups, chans), 1)
-    first = group_c * group_width
-    own = (lane_c >= first) & (lane_c < first + group_width)
-    spread = jnp.where(own, jnp.broadcast_to(mix_f[:, None, :], own.shape), 0.0)
-    spread = spread.astype(bf16).reshape(seqs * groups, chans)
-    drive_re = dot(spread, bb_re).reshape(seqs, groups, states)
-    drive_im = dot(spread, bb_im).reshape(seqs, groups, states)
-    loaded("state", "read", "skip")
-    old_re, old_im = state[0], state[1]
-    new_re = abar_re * old_re - abar_im * old_im + drive_re
-    new_im = abar_re * old_im + abar_im * old_re + drive_im
-    sre_out[...] = new_re
-    sim_out[...] = new_im
-    flat = (seqs * groups, states)
-    readout = lax.dot_general(
-        new_re.reshape(flat).astype(bf16), read_maps[0].astype(bf16), last, preferred_element_type=f32
-    ) - lax.dot_general(
-        new_im.reshape(flat).astype(bf16), read_maps[1].astype(bf16), last, preferred_element_type=f32
-    )
-    readout = jnp.sum(jnp.where(own, readout.reshape(seqs, groups, chans), 0.0), axis=1)
-    pre = readout + skip_ref[...] * mix_f
-    mixer = 0.5 * pre * (1.0 + erf(pre * 0.7071067811865476))
-    mix_all[t] = mixer.astype(bf16)
-    gather(mix_all.at[t], mix_all.at[t], "g1")
-
-    loaded("glu")
-    absorb(mix_all.at[0 : tp - 1], arrival("g1"))
-    glu_gate = jnp.zeros((seqs, chans), f32)
-    for j in range(tp):
-        glu_gate = glu_gate + dot(mix_all[j], glu[j * chans : (j + 1) * chans, :])
-    gated_all[t] = (mixer * jax.nn.sigmoid(glu_gate)).astype(bf16)
-    gather(gated_all.at[t], gated_all.at[t], "g2")
-    loaded("outp", "router")
-    absorb(gated_all.at[0 : tp - 1], arrival("g2"))
-    mixed = resid_ref[...].astype(f32)
-    for j in range(tp):
-        mixed = mixed + dot(gated_all[j], outp[j * chans : (j + 1) * chans, :])
-    stream = mixed.astype(bf16)
-    stream_f = stream.astype(f32)
-
-    tok[0, t, 0:seqs, :] = stream
-    top, bottom = pl.ds(0, half), pl.ds(half, half)
-
-    def slab(n, j, b=0, cut=None):
-        begin, size = b * seqs, seqs
-        if cut is not None:
-            begin, size = begin + cut * half, half
-        return tok.at[n, j, pl.ds(begin, size)]
-
-    def to_twin(n, key, j):
-        remote(slab(n, j, 0), slab(n, j, 1), twin, "twin", ("twin", n, key))
-
-    def spread_chips():
-        for n in range(1, chips):
-            remote(slab(0, t), slab(n, t), (flip(me, 2 * n), t), "chips", ("chips", n))
-
-    def enter(n):
+    held = {}
+    flat = (half * groups, states)
+    read_re, read_im = [], []
+
+    def begin(h):
+        if h == 0:
+            loaded("gains", "proj")
+        absorb(res_all.at[0 : tp - 1, 0:half], arrival(("g0", h)))
+        total = jnp.zeros((half, 1), f32)
+        for j in range(tp):
+            part = res_all[j, halves[h]].astype(f32)
+            total = total + jnp.sum(part * part, axis=1, keepdims=True)
+        scale = lax.rsqrt(total / width + EPSILON)
+        xnorm = [(res_all[j, halves[h]].astype(f32) * scale * gains[0, j]).astype(bf16) for j in range(tp)]
+        mix = dot(jnp.concatenate(xnorm, axis=1), proj[...])
+        mix_f = mix.astype(bf16).astype(f32)
+        lane_c = lax.broadcasted_iota(jnp.int32, (half, groups, chans), 2)
+        group_c = lax.broadcasted_iota(jnp.int32, (half, groups, chans), 1)
+        first = group_c * group_width
+        own = (lane_c >= first) & (lane_c < first + group_width)
+        spread = jnp.where(own, jnp.broadcast_to(mix_f[:, None, :], own.shape), 0.0)
+        spread = spread.astype(bf16).reshape(half * groups, chans)
+        drive_re = dot(spread, bb_re).reshape(half, groups, states)
+        drive_im = dot(spread, bb_im).reshape(half, groups, states)
+        if h == 0:
+            loaded("state", "read", "skip")
+            read_re.append(read_maps[0].astype(bf16))
+            read_im.append(read_maps[1].astype(bf16))
+        old_re, old_im = state[0, halves[h]], state[1, halves[h]]
+        new_re = abar_re * old_re - abar_im * old_im + drive_re
+        new_im = abar_re * old_im + abar_im * old_re + drive_im
+        sre_out[halves[h]] = new_re
+        sim_out[halves[h]] = new_im
+        readout = lax.dot_general(
+            new_re.reshape(flat).astype(bf16), read_re[0], last, preferred_element_type=f32
+        ) - lax.dot_general(
+            new_im.reshape(flat).astype(bf16), read_im[0], last, preferred_element_type=f32
+        )
+        readout = jnp.sum(jnp.where(own, readout.reshape(half, groups, chans), 0.0), axis=1)
+        pre = readout + skip_ref[...] * mix_f
+        mixer = 0.5 * pre * (1.0 + erf(pre * 0.7071067811865476))
+        held["mixer", h] = mixer
+        mix_all[t, halves[h]] = mixer.astype(bf16)
+        gather(mix_all.at[t, halves[h]], mix_all.at[t, halves[h]], "g1", ("g1", h))
+
+    def gate(h):
+        if h == 0:
+            loaded("glu")
+        absorb(mix_all.at[0 : tp - 1, 0:half], arrival(("g1", h)))
+        glu_gate = dot(jnp.concatenate([mix_all[j, halves[h]] for j in range(tp)], axis=1), glu[...])
+        gated_all[t, halves[h]] = (held["mixer", h] * jax.nn.sigmoid(glu_gate)).astype(bf16)
+        gather(gated_all.at[t, halves[h]], gated_all.at[t, halves[h]], "g2", ("g2", h))
+
+    def project(h):
+        if h == 0:
+            loaded("outp", "router")
+        absorb(gated_all.at[0 : tp - 1, 0:half], arrival(("g2", h)))
+        mixed = dot(jnp.concatenate([gated_all[j, halves[h]] for j in range(tp)], axis=1), outp[...])
+        mixed = mixed + resid_ref[halves[h]].astype(f32)
+        tok[0, t, halves[h]] = mixed.astype(bf16)
+        for n in outs[1:]:
+            remote(piece(0, t, h), piece(n, t, h), (flip(me, 2 * n), t), "chips", ("chips", n, h))
+        enter(0, h)
+
+    def piece(n, j, h, b=0):
+        return tok.at[n, j, pl.ds(b * seqs + h * half, half)]
+
+    def to_twin(n, key, j, h):
+        remote(piece(n, j, h), piece(n, j, h, 1), twin, "twin", ("twin", n, key))
+
+    def enter(n, h):
         if n:
-            absorb(home_in.at[0], arrival(("chips", n)))
-        block = slab(n, t)
+            absorb(home_in.at[0, 0:half], arrival(("chips", n, h)))
+        block = piece(n, t, h)
         if n in direct_in:
             remote(block, block, side_o, "relay", ("corner", n))
-        remote(block, block, side_b, "side", ("side", n))
-        remote(block, block, side_a, "side", ("side", n))
-        to_twin(n, "t", t)
-
-    def relay(n):
-        absorb(home_in.at[0:2], arrival(("side", n)))
+        remote(block, block, side_b, "side", ("side", n, h))
+        remote(block, block, side_a, "side", ("side", n, h))
+        to_twin(n, "tba", t, h)
+
+    def relay(n, h):
+        absorb(home_in.at[0:2, 0:half], arrival(("side", n, h)))
         if n not in direct_in:
-            first_b, second_a = slab(n, beside, 0, 0), slab(n, across, 0, 1)
-            remote(first_b, first_b, side_a, "relay", ("corner", n))
-            remote(second_a, second_a, side_b, "relay", ("corner", n))
-        to_twin(n, "ba", beside)
-        to_twin(n, "ba", across)
+            block, peer = (piece(n, beside, 0), side_a) if h == 0 else (piece(n, across, 1), side_b)
+            remote(block, block, peer, "relay", ("corner", n))
+        to_twin(n, "tba", beside, h)
+        to_twin(n, "tba", across, h)
 
     def corner(n):
         absorb(home_in.at[0], arrival(("corner", n)))
-        to_twin(n, "o", opposite)
+        whole = tok.at[n, opposite, pl.ds(0, seqs)]
+        remote(whole, tok.at[n, opposite, pl.ds(seqs, seqs)], twin, "twin", ("twin", n, "o"))
 
     def logits():
+        stream_f = tok[0, t, 0:seqs].astype(f32)
         logit_all[t] = jnp.zeros(logit_all.shape[1:], f32)
         logit_all[t, 0:ep, 0:seqs] = lax.dot_general(
             router_ref[:, pl.ds(pl.multiple_of(t * cols, cols), cols)],
@@ -451,7 +466,7 @@
         logit_all[t, ep : ep + 1, 0:seqs] = jnp.sum(
             jnp.where(row_i == col_i, energy, 0.0), axis=0, keepdims=True
         )
-        gather(logit_all.at[t], logit_all.at[t], "g3")
+        gather(logit_all.at[t], logit_all.at[t], "g3", "g3")
 
     def weights():
         absorb(logit_all.at[0 : tp - 1], arrival("g3"))
@@ -469,18 +484,24 @@
             remote(weight_all.at[0], weight_all.at[k], (flip(me, k), t), "weight", "weight")
 
     def scale_in(n, key):
-        for name, places in (("t", [t]), ("ba", [beside, across]), ("o", [opposite])):
-            if name not in key:
-                continue
-            absorb(res_all.at[0 : len(places)], arrival(("twin", n, name)))
-            for j in places:
-                span = pl.ds(pl.multiple_of(j * cols, cols), cols)
-                ready[n, :, span] = (tok[n, j].astype(f32) * gains[1, j]).astype(bf16)
+        places = {"tba": [t, beside, across], "o": [opposite]}[key]
+        absorb(res_all.at[0 : len(places)], arrival(("twin", n, key)))
+        for j in places:
+            span = pl.ds(pl.multiple_of(j * cols, cols), cols)
+            ready[n, :, span] = (tok[n, j].astype(f32) * gains[1, j]).astype(bf16)
 
     def expert_in(n):
         if n == outs[0]:
             loaded("experts")
         acc[...] = dot(ready[n], wgu[...])
+
+    def expert_gate(n):
+        if n == outs[0]:
+            loaded("experts")
+        acc[:, 0:hidden] = dot(ready[n], wgu[:, 0:hidden])
+
+    def expert_up(n):
+        acc[:, hidden:] = dot(ready[n], wgu[:, hidden:])
 
     def column(line):
         return jnp.sum(jnp.where(row_i == col_i, line, 0.0), axis=1, keepdims=True)
@@ -516,96 +537,86 @@
         mine[n, j] = both
         summed[n, j] = both.astype(bf16)
 
-    def reduce_chip(n):
+    def cut(n, p, side=0):
+        size = half // (2 if n in split_out else 1)
+        return pl.ds(side * half + p * size, size)
+
+    def parts(n):
+        return range(2 if n in split_out else 1)
+
+    def reduce_corner(n):
         if n in early_out:
             absorb(sib_in.at[n, 0], arrival(("corner back", n)))
-            add_twin(n, opposite)
-            if n not in direct_out:
-                remote(summed.at[n, opposite, top], fwd_in.at[n, 0], side_b, "sum", ("fwd", n))
-                remote(summed.at[n, opposite, bottom], fwd_in.at[n, 1], side_a, "sum", ("fwd", n))
+        else:
+            absorb(sib_in.at[n], arrival(("back", n)))
+        add_twin(n, opposite)
+        for p in parts(n):
+            for side, peer in ((0, side_b), (1, side_a)):
+                block = summed.at[n, opposite, cut(n, p, side)]
+                remote(block, fwd_in.at[n, side, cut(n, p)], peer, "sum", ("fwd", n, p))
+
+    def reduce_sides(n):
+        if n in early_out:
+            absorb(sib_in.at[n, 0 : tp - 1], arrival(("back", n)))
+        add_twin(n, beside)
+        add_twin(n, across)
+        for p in parts(n):
+            for side, peer, j in ((0, side_b, beside), (1, side_a, across)):
+                block = summed.at[n, j, cut(n, p, side)]
+                remote(block, from_side.at[n, side, cut(n, p, side)], peer, "sum", ("mine", n, p))
+
+    def reduce_chip(n):
+        reduce_corner(n)
+        reduce_sides(n)
+
+    def reduce_relay(n, p=0):
+        here = cut(n, p)
+        absorb(fwd_in.at[n, :, here], arrival(("fwd", n, p)))
+        for side, peer, j in ((0, side_a, across), (1, side_b, beside)):
+            there = cut(n, p, side)
+            fwd_out[n, side, here] = (mine[n, j, there] + fwd_in[n, side, here].astype(f32)).astype(bf16)
+            remote(fwd_out.at[n, side, here], from_side.at[n, 1 - side, there], peer, "sum", ("mine", n, p))
+
+    def go_home(n, p=0):
+        size = half // len(parts(n))
+        absorb(from_side.at[n, 0:2, 0 : 2 * size], arrival(("mine", n, p)))
+        for side in range(2):
+            there = cut(n, p, side)
+            value = mine[n, t, there] + sib_in[n, t, there].astype(f32)
+            value = value + from_side[n, 0, there].astype(f32) + from_side[n, 1, there].astype(f32)
+            if n:
+                home_out[n, there] = value.astype(bf16)
+                remote(home_out.at[n, there], home_in.at[n, there], (flip(me, 2 * n), t), "home", "home")
             else:
-                remote(summed.at[n, opposite], from_side.at[n, 2], side_o, "sum", ("mine", n))
-            absorb(sib_in.at[n, 0 : tp - 1], arrival(("back", n)))
-            add_twin(n, beside)
-            add_twin(n, across)
-            if n in direct_out:
-                remote(summed.at[n, beside], from_side.at[n, 0], side_b, "sum", ("mine", n))
-                remote(summed.at[n, across], from_side.at[n, 1], side_a, "sum", ("mine", n))
-            else:
-                remote(summed.at[n, beside, top], from_side.at[n, 0, top], side_b, "sum", ("mine", n))
-                remote(summed.at[n, across, bottom], from_side.at[n, 1, bottom], side_a, "sum", ("mine", n))
-            return
-        absorb(sib_in.at[n], arrival(("back", n)))
-        for j in (opposite, beside, across):
-            add_twin(n, j)
-        if n in direct_out:
-            remote(summed.at[n, opposite], from_side.at[n, 2], side_o, "sum", ("mine", n))
-            remote(summed.at[n, beside], from_side.at[n, 0], side_b, "sum", ("mine", n))
-            remote(summed.at[n, across], from_side.at[n, 1], side_a, "sum", ("mine", n))
-            return
-        remote(summed.at[n, opposite, top], fwd_in.at[n, 0], side_b, "sum", ("fwd", n))
-        remote(summed.at[n, opposite, bottom], fwd_in.at[n, 1], side_a, "sum", ("fwd", n))
-        remote(summed.at[n, beside, top], from_side.at[n, 0, top], side_b, "sum", ("mine", n))
-        remote(summed.at[n, across, bottom], from_side.at[n, 1, bottom], side_a, "sum", ("mine", n))
-
-    def reduce_relay(n):
-        if n in direct_out:
-            return
-        absorb(fwd_in.at[n], arrival(("fwd", n)))
-        fwd_out[n, 0] = (mine[n, across, 0:half] + fwd_in[n, 0].astype(f32)).astype(bf16)
-        fwd_out[n, 1] = (mine[n, beside, half:] + fwd_in[n, 1].astype(f32)).astype(bf16)
-        remote(fwd_out.at[n, 0], from_side.at[n, 1, top], side_a, "sum", ("mine", n))
-        remote(fwd_out.at[n, 1], from_side.at[n, 0, bottom], side_b, "sum", ("mine", n))
-
-    def go_home(n):
-        value = mine[n, t] + sib_in[n, t].astype(f32)
-        count = 3 if n in direct_out else 2
-        absorb(from_side.at[n, 0:count], arrival(("mine", n)))
-        for k in range(count):
-            value = value + from_side[n, k].astype(f32)
-        if n:
-            home_out[n] = value.astype(bf16)
-            remote(home_out.at[n], home_in.at[n], (flip(me, 2 * n), t), "home", "home")
-        else:
-            mine[n, t] = value
+                mine[n, t, there] = value
 
     def finish():
-        result = stream_f + mine[0, t]
+        result = tok[0, t, 0:seqs].astype(f32) + mine[0, t]
         absorb(home_in.at[0 : chips - 1], arrival("home"))
         for n in range(1, chips):
             result = result + home_in[n].astype(f32)
         out_ref[...] = result.astype(bf16)
 
-    direct_in, direct_out = (), ()
-    outs, early_out = (0, 1, 2, 3), (3,)
+    outs, early_out, split_out, direct_in = (0, 1, 2, 3), (3,), (), ()
     plan = [
-        (spread_chips,), (enter, 0), (logits,),
-        (relay, 0), (enter, 1), (enter, 2), (weights,), (scale_in, 0, "t"), (corner, 0), (scale_in, 0, "ba"), (scale_in, 1, "t"), (relay, 1), (enter, 3),
-        (scale_in, 0, "o"), (expert_in, 0), (relay, 2), (activate, 0), (scale_in, 1, "ba"), (corner, 1), (expert_out, 0), (relay, 3), (scale_in, 2, "t"), (scale_in, 2, "ba"), (scale_in, 1, "o"),
-        (expert_in, 1), (corner, 2), (reduce_chip, 0), (activate, 1), (expert_out, 1), (scale_in, 3, "t"), (corner, 3), (scale_in, 3, "ba"),
+        (begin, 0), (begin, 1), (gate, 0), (gate, 1), (project, 0), (project, 1), (logits,), (relay, 0, 0),
+        (enter, 1, 0), (relay, 0, 1), (enter, 1, 1), (enter, 2, 0), (enter, 2, 1), (weights,), (relay, 1, 0),
+        (corner, 0), (scale_in, 0, "tba"), (relay, 1, 1), (enter, 3, 0), (enter, 3, 1), (scale_in, 0, "o"),
+        (expert_in, 0), (relay, 2, 0), (relay, 2, 1), (activate, 0), (scale_in, 1, "tba"), (corner, 1),
+        (expert_out, 0), (relay, 3, 0), (relay, 3, 1), (scale_in, 2, "tba"), (scale_in, 1, "o"), (expert_in, 1),
+        (corner, 2), (reduce_chip, 0), (activate, 1), (expert_out, 1), (corner, 3), (scale_in, 3, "tba"),
         (scale_in, 2, "o"), (expert_in, 2), (reduce_chip, 1), (activate, 2), (expert_out, 2), (reduce_relay, 0),
-        (scale_in, 3, "o"), (expert_in, 3), (reduce_chip, 2), (activate, 3), (expert_out, 3), (reduce_relay, 1), (go_home, 0),
-        (reduce_chip, 3), (reduce_relay, 2), (go_home, 1), (reduce_relay, 3), (go_home, 2), (go_home, 3),
-        (finish,),
+        (scale_in, 3, "o"), (expert_in, 3), (reduce_chip, 2), (activate, 3), (expert_out, 3), (reduce_relay, 1),
+        (go_home, 0), (reduce_chip, 3), (reduce_relay, 2), (go_home, 1), (reduce_relay, 3), (go_home, 2),
+        (go_home, 3), (finish,),
     ]
     for step in plan:
         step[0](*step[1:])
-    spent = {
-        "g0": res_all.at[0 : tp - 1],
-        "g1": mix_all.at[0 : tp - 1],
-        "g2": gated_all.at[0 : tp - 1],
-        "g3": logit_all.at[0 : tp - 1],
-        "weight": weight_all.at[0 : ep - 1],
-        "chips": home_in.at[0 : chips - 1],
-        "side": tok.at[0],
-        "relay": tok.at[0, 0 : tp // 2],
-        "twin": tok.at[0:2],
-        "back": sib_in,
-        "home": home_in.at[0 : chips - 1],
-    }
-    for kind, ref in spent.items():
-        absorb(ref, send_sem.at[SENDS.index(kind)])
-    absorb(sib_in.at[:, 0:3], send_sem.at[SENDS.index("sum")])
+    block = seqs * cols
+    sent = 3 * block + 6 * seqs * chans + (chips - 1) * 2 * block + chips * (2 + 1 + 4 + 4 + 3) * block
+    absorb(wgu.at[0 : sent // (2 * hidden)], send_sem.at[SENDS.index("rows")])
+    absorb(logit_all.at[0 : tp - 1], send_sem.at[SENDS.index("g3")])
+    absorb(weight_all.at[0 : ep - 1], send_sem.at[SENDS.index("weight")])
 
 
 def finish_kernel(a_in, b_in, c_in, a_out, b_out, c_out, sems):
@@ -685,7 +696,7 @@
             pltpu.VMEM((chips, seqs, cols), bf16),
             pltpu.SemaphoreType.DMA((15,)),
             pltpu.SemaphoreType.DMA((len(SENDS),)),
-            pltpu.SemaphoreType.DMA((42,)),
+            pltpu.SemaphoreType.DMA((34,)),
         ],
         compiler_params=pltpu.CompilerParams(
             collective_id=0, has_side_effects=True, vmem_limit_bytes=48 * 1024 * 1024

time: 52.5 us -> 50.7 us (0.966)
  Pallas kernels: 51.7 us -> 49.9 us
    pallas_call x1, Pallas kernels: 50.7 us -> 48.9 us  [dispatch(): pl.pallas_call(functools.partial(layer_kernel, (ep, tp)), out_shape=(pltp...]
where the time goes in v4:
time: 50.7 us; the launch traced here: 50.6 us
  Pallas kernels  49.9 us (98%)
  between operations  0.65 us (1%)
    pallas_call x1, Pallas kernels, dispatch(): pl.pallas_call(functools.partial(layer_kernel, (ep, tp)), out_shape=(pltp...  48.9 us
    pallas_call x1, Pallas kernels, dispatch(): pl.pallas_call(finish_kernel, out_shape=tuple((jax.ShapeDtypeStruct(part....  1.02 us

profile of v4, /device:TPU:0, one launch (start us, length us, event | category | flops | bytes accessed | tf_op | source)
XLA Modules:
  0.0 50.6 jit_solution(15641415667864168310)
XLA Ops:
  0.6 48.9 %layer.1 = (bf16[64,512]{1,0:T(8,128)(2,1)S(1)}, f32[64,16,64]{2,1,0:T(8,128)S(1)}, f32[64,16,64]{2,1,0:T(8,128)S(1)}) custom-call(bf16[64,512]{1,0:T(8,128)(2,1)} %resid_hbm.1, f32[4,1,512]{2,1,0:T(1,128)} %bitcast.21, f32[4,1,512]{2,1,0:T(1,128)} %bitcast.22, f32[16,64]{1,0:T(8,128)} %decay_hbm.1, f32[16,64]{1,0:T(8,128)} %freq_hbm.1, f32[1,16]{1,0:T(1,128)} %bitcast.25, ...), custom_call_target="tpu_custom_call" | custom-call | tf_op jit(solution)/shard_map/layer/pallas_call | solution.py:654
  49.6 1.0 %finish.1 = (bf16[64,512]{1,0:T(8,128)(2,1)}, f32[64,16,64]{2,1,0:T(8,128)}, f32[64,16,64]{2,1,0:T(8,128)}) custom-call(bf16[64,512]{1,0:T(8,128)(2,1)S(1)} %get-tuple-element.6.a_in, f32[64,16,64]{2,1,0:T(8,128)S(1)} %get-tuple-element.7.b_in, f32[64,16,64]{2,1,0:T(8,128)S(1)} %get-tuple-element.8.c_in), custom_call_target="tpu_custom_call" | custom-call | tf_op jit(solution)/shard_map/finish/pallas_call | solution.py:728

commit v5 on v4

--- a/solution.py
+++ b/solution.py
@@ -213,7 +213,6 @@
     weight_all,
     tok,
     ready,
-    acc,
     act,
     mine,
     sib_out,
@@ -229,7 +228,6 @@
     recv_sem,
 ):
     ep, tp = sizes
-    rows = 2 * resid_ref.shape[0]
     f32, bf16 = jnp.float32, jnp.bfloat16
     me, t = lax.axis_index("ep"), lax.axis_index("tp")
     seqs, cols = resid_ref.shape
@@ -240,6 +238,7 @@
     chips = ep // 2
     half = seqs // 2
     hidden = wd.shape[1]
+    piece_cols = 512
     last = (((1,), (1,)), ((), ()))
 
     def dot(a, b):
@@ -490,32 +489,25 @@
             span = pl.ds(pl.multiple_of(j * cols, cols), cols)
             ready[n, :, span] = (tok[n, j].astype(f32) * gains[1, j]).astype(bf16)
 
-    def expert_in(n):
+    def column(line):
+        return jnp.sum(jnp.where(row_i == col_i, line, 0.0), axis=1, keepdims=True)
+
+    def expert(n):
         if n == outs[0]:
             loaded("experts")
-        acc[...] = dot(ready[n], wgu[...])
-
-    def expert_gate(n):
-        if n == outs[0]:
-            loaded("experts")
-        acc[:, 0:hidden] = dot(ready[n], wgu[:, 0:hidden])
-
-    def expert_up(n):
-        acc[:, hidden:] = dot(ready[n], wgu[:, hidden:])
-
-    def column(line):
-        return jnp.sum(jnp.where(row_i == col_i, line, 0.0), axis=1, keepdims=True)
-
-    def activate(n):
-        if n == outs[0]:
             absorb(weight_all.at[0 : ep - 1], arrival("weight"))
+        norm, share = [], []
         for b in range(2):
-            lines = slice(b * seqs, (b + 1) * seqs)
-            norm = column(weight_all[2 * n + b, ep : ep + 1, 0:seqs])
-            share = column(weight_all[2 * n + b, pl.ds(me, 1), 0:seqs])
-            gate_cl = jnp.minimum(acc[lines, 0:hidden] * norm, LIMIT)
-            up_cl = jnp.clip(acc[lines, hidden:] * norm, -LIMIT, LIMIT)
-            act[n, lines] = (((up_cl + 1.0) * share) * (gate_cl * jax.nn.sigmoid(ALPHA * gate_cl))).astype(bf16)
+            norm.append(column(weight_all[2 * n + b, ep : ep + 1, 0:seqs]))
+            share.append(column(weight_all[2 * n + b, pl.ds(me, 1), 0:seqs]))
+        norm, share = jnp.concatenate(norm, axis=0), jnp.concatenate(share, axis=0)
+        for c in range(0, hidden, piece_cols):
+            gate_pre = dot(ready[n], wgu[:, c : c + piece_cols])
+            up_pre = dot(ready[n], wgu[:, hidden + c : hidden + c + piece_cols])
+            gate_cl = jnp.minimum(gate_pre * norm, LIMIT)
+            up_cl = jnp.clip(up_pre * norm, -LIMIT, LIMIT)
+            value = ((up_cl + 1.0) * share) * (gate_cl * jax.nn.sigmoid(ALPHA * gate_cl))
+            act[n, :, c : c + piece_cols] = value.astype(bf16)
 
     def expert_out(n):
         if n == outs[0]:
@@ -600,15 +592,14 @@
     outs, early_out, split_out, direct_in = (0, 1, 2, 3), (3,), (), ()
     plan = [
         (begin, 0), (begin, 1), (gate, 0), (gate, 1), (project, 0), (project, 1), (logits,), (relay, 0, 0),
-        (enter, 1, 0), (relay, 0, 1), (enter, 1, 1), (enter, 2, 0), (enter, 2, 1), (weights,), (relay, 1, 0),
+        (enter, 1, 0), (relay, 0, 1), (enter, 1, 1), (weights,), (enter, 2, 0), (enter, 2, 1), (relay, 1, 0),
         (corner, 0), (scale_in, 0, "tba"), (relay, 1, 1), (enter, 3, 0), (enter, 3, 1), (scale_in, 0, "o"),
-        (expert_in, 0), (relay, 2, 0), (relay, 2, 1), (activate, 0), (scale_in, 1, "tba"), (corner, 1),
-        (expert_out, 0), (relay, 3, 0), (relay, 3, 1), (scale_in, 2, "tba"), (scale_in, 1, "o"), (expert_in, 1),
-        (corner, 2), (reduce_chip, 0), (activate, 1), (expert_out, 1), (corner, 3), (scale_in, 3, "tba"),
-        (scale_in, 2, "o"), (expert_in, 2), (reduce_chip, 1), (activate, 2), (expert_out, 2), (reduce_relay, 0),
-        (scale_in, 3, "o"), (expert_in, 3), (reduce_chip, 2), (activate, 3), (expert_out, 3), (reduce_relay, 1),
-        (go_home, 0), (reduce_chip, 3), (reduce_relay, 2), (go_home, 1), (reduce_relay, 3), (go_home, 2),
-        (go_home, 3), (finish,),
+        (expert, 0), (relay, 2, 0), (relay, 2, 1), (scale_in, 1, "tba"), (corner, 1), (expert_out, 0),
+        (relay, 3, 0), (relay, 3, 1), (scale_in, 2, "tba"), (scale_in, 1, "o"), (expert, 1), (corner, 2),
+        (reduce_chip, 0), (expert_out, 1), (corner, 3), (scale_in, 3, "tba"), (scale_in, 2, "o"), (expert, 2),
+        (reduce_chip, 1), (expert_out, 2), (reduce_relay, 0), (scale_in, 3, "o"), (expert, 3), (reduce_chip, 2),
+        (expert_out, 3), (reduce_relay, 1), (go_home, 0), (reduce_chip, 3), (reduce_relay, 2), (go_home, 1),
+        (reduce_relay, 3), (go_home, 2), (go_home, 3), (finish,),
     ]
     for step in plan:
         step[0](*step[1:])
@@ -683,7 +674,6 @@
             pltpu.VMEM((ep, 2 * ep, 128), f32),
             pltpu.VMEM((chips, tp, 2 * seqs, cols), bf16),
             pltpu.VMEM((chips, 2 * seqs, width), bf16),
-            pltpu.VMEM((2 * seqs, 2 * hidden), f32),
             pltpu.VMEM((chips, 2 * seqs, hidden), bf16),
             pltpu.VMEM(blocks, f32),
             pltpu.VMEM(blocks, bf16),

time: 50.7 us -> 51 us (level)
  no operation moved by 1% of the time
where the time goes in v5:
time: 51 us; the launch traced here: 50.8 us
  Pallas kernels  50.2 us (98%)
  between operations  0.65 us (1%)
    pallas_call x1, Pallas kernels, dispatch(): pl.pallas_call(functools.partial(layer_kernel, (ep, tp)), out_shape=(pltp...  49.2 us

profile of v5, /device:TPU:0, one launch (start us, length us, event | category | flops | bytes accessed | tf_op | source)
XLA Modules:
  0.0 50.8 jit_solution(10623228674259911617)
XLA Ops:
  0.6 49.2 %layer.1 = (bf16[64,512]{1,0:T(8,128)(2,1)S(1)}, f32[64,16,64]{2,1,0:T(8,128)S(1)}, f32[64,16,64]{2,1,0:T(8,128)S(1)}) custom-call(bf16[64,512]{1,0:T(8,128)(2,1)} %resid_hbm.1, f32[4,1,512]{2,1,0:T(1,128)} %bitcast.21, f32[4,1,512]{2,1,0:T(1,128)} %bitcast.22, f32[16,64]{1,0:T(8,128)} %decay_hbm.1, f32[16,64]{1,0:T(8,128)} %freq_hbm.1, f32[1,16]{1,0:T(1,128)} %bitcast.25, ...), custom_call_target="tpu_custom_call" | custom-call | tf_op jit(solution)/shard_map/layer/pallas_call | solution.py:645
  49.8 1.0 %finish.1 = (bf16[64,512]{1,0:T(8,128)(2,1)}, f32[64,16,64]{2,1,0:T(8,128)}, f32[64,16,64]{2,1,0:T(8,128)}) custom-call(bf16[64,512]{1,0:T(8,128)(2,1)S(1)} %get-tuple-element.6.a_in, f32[64,16,64]{2,1,0:T(8,128)S(1)} %get-tuple-element.7.b_in, f32[64,16,64]{2,1,0:T(8,128)S(1)} %get-tuple-element.8.c_in), custom_call_target="tpu_custom_call" | custom-call | tf_op jit(solution)/shard_map/finish/pallas_call | solution.py:718
